TPU v7x, 32 devices: a whole 2x2x4 slice. The times are simulated.
32 devices in a mesh: rep: 2 (over x), fs: 8 (over z, y), tp: 2 (over core).
Axes of the slice: x: 2, y: 2, z: 4, core: 2. Of those that a mesh axis runs over, the one named last changes fastest.
Arguments:
- tokens: bfloat16 [12288, 2048], P(('rep', 'fs', 'tp')), may hold values from -6 to 6
- outer_weight: float32 [2048, 1536], P('fs', 'tp'), may hold values from -0.125 to 0.125
- inner_weight: float32 [2048, 1536], P('fs', 'tp'), may hold values from -0.125 to 0.125
- value_weight: float32 [2048, 1536], P('fs', 'tp'), may hold values from -0.125 to 0.125
- conv_taps: float32 [3, 1536], P(None, 'tp'), may hold values from -3 to 3
- mix_out: float32 [1536, 2048], P('tp', 'fs'), may hold values from -0.15625 to 0.15625
- norm_first: float32 [2048], replicated, may hold values from 0.1 to 1.9
- up_weight: float32 [2048, 4096], P('fs', 'tp'), may hold values from -0.125 to 0.125
- down_weight: float32 [4096, 2048], P('tp', 'fs'), may hold values from -0.09375 to 0.09375
- norm_second: float32 [2048], replicated, may hold values from 0.1 to 1.9
Outputs:
- encoded: bfloat16 [12288, 2048], P(('rep', 'fs', 'tp'))
All inputs are finite; a program needn't handle non-finite values.
Results may differ from a plain program's by a relative error of at most 0.015.
Values may be sent and summed in bfloat16 or wider, within the bound.
A program may use at most 128 MiB of HBM per device.

v0:
```python
import functools

import jax
import jax.numpy as jnp
from jax import lax
from jax.experimental import pallas as pl
from jax.experimental.pallas import tpu as pltpu
from jax.sharding import PartitionSpec as P

SEQ = 128


residual_scale = 2.0**0.25
norm_epsilon = 1e-05


def layer_norm(values, scaling):
    center = values - jnp.mean(values, axis=-1, keepdims=True)
    spread = jnp.mean(center * center, axis=-1, keepdims=True)
    return center * lax.rsqrt(spread + norm_epsilon) * scaling


def short_conv(product, conv_taps):
    places = jnp.arange(product.shape[0], dtype=jnp.int32) % SEQ
    blank = jnp.zeros((1, product.shape[1]), jnp.float32)
    before = jnp.concatenate([blank, product[:-1]], axis=0)
    after = jnp.concatenate([product[1:], blank], axis=0)
    before = jnp.where((places > 0)[:, None], before, 0.0)
    after = jnp.where((places < SEQ - 1)[:, None], after, 0.0)
    return conv_taps[0] * before + conv_taps[1] * product + conv_taps[2] * after


def local(
    tokens,
    outer_weight,
    inner_weight,
    value_weight,
    conv_taps,
    mix_out,
    norm_first,
    up_weight,
    down_weight,
    norm_second,
):
    grouped = lax.all_gather(tokens, "tp", axis=0, tiled=True)
    outer_bf = outer_weight.astype(jnp.bfloat16)
    inner_bf = inner_weight.astype(jnp.bfloat16)
    value_bf = value_weight.astype(jnp.bfloat16)
    outer_full, inner_full, value_full = (
        lax.all_gather(outer_bf, "fs", axis=0, tiled=True),
        lax.all_gather(inner_bf, "fs", axis=0, tiled=True),
        lax.all_gather(value_bf, "fs", axis=0, tiled=True),
    )
    outer = jnp.dot(grouped, outer_full, preferred_element_type=jnp.float32)
    inner = jnp.dot(grouped, inner_full, preferred_element_type=jnp.float32)
    value = jnp.dot(grouped, value_full, preferred_element_type=jnp.float32)
    mixed = (outer * short_conv(inner * value, conv_taps)).astype(jnp.bfloat16)
    mixout_full = lax.all_gather(mix_out.astype(jnp.bfloat16), "fs", axis=1, tiled=True)
    selected = mixed
    mixing = lax.psum_scatter(
        jnp.dot(selected, mixout_full, preferred_element_type=jnp.float32).astype(jnp.bfloat16),
        "tp",
        scatter_dimension=0,
        tiled=True,
    ).astype(jnp.float32)
    first = layer_norm(residual_scale * tokens.astype(jnp.float32) + mixing, norm_first).astype(
        jnp.bfloat16
    )
    grouped_first = lax.all_gather(first, "tp", axis=0, tiled=True)
    upward_bf = up_weight.astype(jnp.bfloat16)
    upward_full = lax.all_gather(upward_bf, "fs", axis=0, tiled=True)
    raised = jnp.dot(grouped_first, upward_full, preferred_element_type=jnp.float32)
    raised = jax.nn.relu(raised)
    hidden = (raised * raised).astype(jnp.bfloat16)
    down_full = lax.all_gather(down_weight.astype(jnp.bfloat16), "fs", axis=1, tiled=True)
    selected = hidden
    lowered = lax.psum_scatter(
        jnp.dot(selected, down_full, preferred_element_type=jnp.float32).astype(jnp.bfloat16),
        "tp",
        scatter_dimension=0,
        tiled=True,
    ).astype(jnp.float32)
    return layer_norm(residual_scale * first.astype(jnp.float32) + lowered, norm_second).astype(
        jnp.bfloat16
    )


MESH = pl.DeviceIdType.MESH
BF = jnp.bfloat16
F32 = jnp.float32


def dot(a, b):
    return jnp.dot(a, b, preferred_element_type=F32)


def layer_kernel(
    n,
    tokens_hbm,
    outer_hbm,
    inner_hbm,
    value_hbm,
    taps_ref,
    mix_hbm,
    norm1_ref,
    up_hbm,
    down_hbm,
    norm2_ref,
    out_ref,
    wa,
    wb,
    wc,
    wd,
    tok,
    acc,
    mixed,
    own,
    psend,
    precv1,
    precv2,
    xsend,
    xrecv,
    fst,
    hid,
    load_sem,
    ring_send,
    ring_recv,
    tp_send,
    tp_recv,
    x_send,
    x_recv,
):
    half = n // 2
    r = lax.axis_index("rep")
    f = lax.axis_index("fs")
    t = lax.axis_index("tp")
    rows = tokens_hbm.shape[0]
    both = 2 * rows
    d = tokens_hbm.shape[1]
    ks = wa.shape[2]
    wch = wa.shape[3]
    ff = wc.shape[1]
    nc = wb.shape[2]

    odd = f % 2
    pos = (1 - odd) * (f // 2) + odd * (n - 1 - f // 2)

    def at(place):
        p = (place + 2 * n) % n
        hi = p // half
        return (1 - hi) * (2 * p) + hi * (2 * (n - 1 - p) + 1)

    right = {"fs": at(pos + 1)}
    left = {"fs": at(pos - 1)}
    across = {"rep": 1 - r}
    mate = {"tp": 1 - t}

    mine = pl.multiple_of(r * ff, 128)
    first_down = min(ff, both)
    rest_down = ff - first_down
    loads = [
        pltpu.make_async_copy(
            src, acc.at[pl.ds(i * ks, ks), pl.ds(0, wch)], load_sem.at[i]
        )
        for i, src in enumerate((outer_hbm, inner_hbm, value_hbm))
    ]
    loads += [
        pltpu.make_async_copy(mix_hbm, own.at[0, pl.ds(0, wch)], load_sem.at[3]),
        pltpu.make_async_copy(
            up_hbm.at[:, pl.ds(mine, ff)],
            acc.at[pl.ds(3 * ks, ks), pl.ds(0, ff)],
            load_sem.at[4],
        ),
        pltpu.make_async_copy(
            down_hbm.at[pl.ds(mine, first_down)],
            own.at[1, pl.ds(0, first_down)],
            load_sem.at[5],
        ),
        pltpu.make_async_copy(tokens_hbm, tok.at[pl.ds(0, rows)], load_sem.at[6]),
    ]
    if rest_down:
        loads.append(
            pltpu.make_async_copy(
                down_hbm.at[pl.ds(mine + first_down, rest_down)],
                own.at[2, pl.ds(0, rest_down)],
                load_sem.at[7],
            )
        )
    for load in loads[:3]:
        load.start()

    barrier = pltpu.get_barrier_semaphore()
    for device in (right, left, across, mate):
        pl.semaphore_signal(barrier, inc=1, device_id=device, device_id_type=MESH)
    pl.semaphore_wait(barrier, 4)

    def mate_copy(i, src, dst):
        return pltpu.make_async_remote_copy(
            src_ref=src,
            dst_ref=dst,
            send_sem=tp_send.at[i],
            recv_sem=tp_recv.at[i],
            device_id=mate,
            device_id_type=MESH,
        )

    def across_copy(i, src, dst):
        return pltpu.make_async_remote_copy(
            src_ref=src,
            dst_ref=dst,
            send_sem=x_send.at[i],
            recv_sem=x_recv.at[i],
            device_id=across,
            device_id_type=MESH,
        )

    def piece(ti, which, owner):
        if ti == 0:
            return wa.at[2 if which else r, owner]
        if ti == 1:
            u = wch // 64 * 16
            if which:
                return wb.at[owner, pl.ds(2 * u, wch - 2 * u)]
            return wb.at[owner, pl.ds(pl.multiple_of(r * u, 16), u)]
        if ti == 2:
            u = ks // 2
            return wc.at[pl.ds(pl.multiple_of(owner * ks + which * u, 16), u)]
        return wd.at[owner, pl.ds(which * (ff // 2), ff // 2)]

    per = 6 * half - 3
    index = {}
    for h in range(1, half + 1):
        for kind in ("Rq", "Rp", "Lq", "Lp", "XR", "XL"):
            if h == half and kind in ("Rp", "Lq", "XL"):
                continue
            index[kind, h] = len(index)

    copies = {}

    def message(ti, kind, h):
        key = (ti, kind, h)
        if key not in copies:
            which = int(kind[1] == "p")
            if kind[0] == "R":
                src, device = at(pos - (h - 1)), right
            elif kind[0] == "L":
                src, device = at(pos + (h - 1)), left
            else:
                src, device = at(pos - h if kind == "XR" else pos + h), across
            i = ti * per + index[kind, h]
            ref = piece(ti, which, src)
            copies[key] = pltpu.make_async_remote_copy(
                src_ref=ref,
                dst_ref=ref,
                send_sem=ring_send.at[i],
                recv_sem=ring_recv.at[i],
                device_id=device,
                device_id_type=MESH,
            )
        return copies[key]

    def send(ti, kind, h):
        if ti < 4 and (kind, h) in index and (ti < 2 or kind[0] != "X"):
            message(ti, kind, h).start()

    def got(ti, kind, h):
        message(ti, kind, h).wait_recv()

    def event(ti, h, which):
        if which == 0:
            got(ti, "Rq", h)
            send(ti, "Rq", h + 1)
            send(ti, "XR", h)
            if h == half:
                send(ti + 1, "Rp", 1)
            got(ti, "Lp", h)
            send(ti, "Lp", h + 1)
            if h == half:
                send(ti + 1, "Lq", 1)
        else:
            got(ti, "Rp", h)
            if h + 1 < half:
                send(ti, "Rp", h + 1)
            else:
                send(ti + 1, "Rq", 1)
            got(ti, "Lq", h)
            if h + 1 < half:
                send(ti, "Lq", h + 1)
            else:
                send(ti + 1, "Lp", 1)
            send(ti, "XL", h)

    def events(ti):
        out = []
        for h in range(1, half + 1):
            out.append((ti, h, 0))
            if h < half:
                out.append((ti, h, 1))
        return out

    def arrived(ti, h):
        got(ti, "XR", h)
        if h < half:
            got(ti, "XL", h)

    def owners(h):
        if h == 0:
            return [f]
        if h == half:
            return [at(pos + half)]
        return [at(pos - h), at(pos + h)]

    for i in range(3):
        loads[i].wait()
        wa[i, f] = acc[pl.ds(i * ks, ks), pl.ds(0, wch)].astype(BF)
    send(0, "Rq", 1)
    send(0, "Lp", 1)
    send(0, "Rp", 1)
    send(0, "Lq", 1)
    for load in loads[3:]:
        load.start()
    share = mate_copy(0, tokens_hbm, tok.at[pl.ds(rows, rows)])
    share.start()
    loads[3].wait()
    wb[f] = own[0, pl.ds(0, wch)].astype(BF)
    loads[4].wait()
    wc[pl.ds(pl.multiple_of(f * ks, 16), ks), :] = acc[
        pl.ds(3 * ks, ks), pl.ds(0, ff)
    ].astype(BF)
    loads[5].wait()
    wd[f, pl.ds(0, first_down)] = own[1, pl.ds(0, first_down)].astype(BF)
    if rest_down:
        loads[7].wait()
        wd[f, pl.ds(first_down, rest_down)] = own[2, pl.ds(0, rest_down)].astype(BF)
    loads[6].wait()
    share.wait_recv()

    tn = 256
    pieces = 4
    pr = rows // pieces
    mix_sem, first_sem = 1, 1 + n
    diag_sem = first_sem + pieces
    far_sem = diag_sem + pieces
    near_sem = far_sem + n
    OWN, TWIN, MATE, DIAG = 0, rows, 2 * rows, 3 * rows

    def accumulate(x_ref, gap, h, weight, width, dest):
        who = owners(h)

        def unit(i, _):
            side = i % 2
            c = i // 2
            total = None
            for o in who:
                x = x_ref[
                    pl.ds(pl.multiple_of(side * gap, 16), rows),
                    pl.ds(pl.multiple_of(o * ks, 128), ks),
                ]
                term = dot(x, weight(o, pl.ds(pl.multiple_of(c * tn, tn), tn)))
                total = term if total is None else total + term
            view = dest(pl.multiple_of(side * rows, 16), c)
            if h == 0:
                view[...] = total
            else:
                view[...] += total
            return 0

        lax.fori_loop(0, 2 * (width // tn), unit, 0)

    def acc_at(base):
        def dest(m, c):
            return acc.at[
                pl.ds(base + m, rows), pl.ds(pl.multiple_of(c * tn, tn), tn)
            ]

        return dest

    def project(h, tensors=(0, 1, 2)):
        for i in tensors:
            dest = (
                acc_at(i * both)
                if i < 2
                else lambda m, c: own.at[c, pl.ds(m, rows), :]
            )
            accumulate(tok, rows, h, lambda o, c, i=i: wa[i, o, :, c], wch, dest)

    def raise_part(size, start, x_base, acc_base, hs, new, final):
        who = [o for h in hs for o in owners(h)]
        tiles = ff // tn

        def unit(i, _):
            side = i % 2
            c = pl.ds(pl.multiple_of(i // 2 * tn, tn), tn)
            x_row = pl.multiple_of(x_base + side * MATE + start, 16)
            total = None
            for o in who:
                x = fst[
                    pl.ds(x_row, size), pl.ds(pl.multiple_of(o * ks, 128), ks)
                ]
                term = dot(x, wc[pl.ds(pl.multiple_of(o * ks, 16), ks), c])
                total = term if total is None else total + term
            span = pl.ds(pl.multiple_of(acc_base + side * rows + start, 16), size)
            if not new:
                total = total + acc[span, c]
            if final:
                total = jnp.maximum(total, 0.0)
                hid[pl.ds(x_row, size), c] = (total * total).astype(BF)
            else:
                acc[span, c] = total
            return 0

        lax.fori_loop(0, 2 * tiles, unit, 0)

    def raise_near(h):
        raise_part(rows, 0, OWN, 0, [h], h == 0, h == half)

    def raise_far(p, count, hs):
        raise_part(pr * count, p * pr, TWIN, both, hs, 0 in hs, half in hs)

    def numbered(h):
        return [(0 if h == 0 else 2 * h - 1 + k, o) for k, o in enumerate(owners(h))]

    every = [item for h in range(half + 1) for item in numbered(h)]

    def mix_block(k, o):
        return mate_copy(mix_sem + k, psend.at[o, pl.ds(0, rows)], precv1.at[o])

    def near_block(k, o):
        part = pl.ds(0, rows)
        return mate_copy(near_sem + k, psend.at[o, part], precv2.at[o, part])

    def far_block(k, o):
        part = pl.ds(rows, rows)
        return mate_copy(far_sem + k, psend.at[o, part], precv2.at[o, part])

    def across_block(k, o):
        return across_copy(pieces + k, xsend.at[o], xrecv.at[o])

    def mixout(h):
        for k, o in numbered(h):
            psend[o, pl.ds(0, rows)] = dot(mixed[pl.ds(rows, rows), :], wb[o]).astype(BF)
            mix_block(k, o).start()
            own[o, pl.ds(0, rows)] = dot(mixed[pl.ds(0, rows), :], wb[o])

    def lower_far(h):
        for k, o in numbered(h):
            psend[o, pl.ds(rows, rows)] = dot(hid[pl.ds(DIAG, rows), :], wd[o]).astype(BF)
            far_block(k, o).start()
            own[o, pl.ds(rows, rows)] = dot(hid[pl.ds(TWIN, rows), :], wd[o])

    def pass_across(h):
        for k, o in numbered(h):
            far_block(k, o).wait_recv()
            part = pl.ds(rows, rows)
            xsend[o] = (own[o, part] + precv2[o, part].astype(F32)).astype(BF)
            across_block(k, o).start()

    def lower_near(h):
        for k, o in numbered(h):
            psend[o, pl.ds(0, rows)] = dot(hid[pl.ds(MATE, rows), :], wd[o]).astype(BF)
            near_block(k, o).start()
            own[o, pl.ds(0, rows)] = dot(hid[pl.ds(OWN, rows), :], wd[o])

    def mix():
        seq = SEQ

        def unit(i, _):
            m = pl.multiple_of((i % (both // seq)) * seq, seq)
            c = pl.multiple_of((i // (both // seq)) * tn, tn)
            o = acc[pl.ds(m, seq), pl.ds(c, tn)]
            p = (
                acc[pl.ds(both + m, seq), pl.ds(c, tn)]
                * own[i // (both // seq), pl.ds(m, seq), :]
            )
            place = lax.broadcasted_iota(jnp.int32, p.shape, 0)
            before = jnp.where(place > 0, pltpu.roll(p, 1, 0), 0.0)
            after = jnp.where(place < seq - 1, pltpu.roll(p, seq - 1, 0), 0.0)
            taps = taps_ref[:, pl.ds(c, tn)]
            conv = taps[0:1] * before + taps[1:2] * p + taps[2:3] * after
            mixed[pl.ds(m, seq), pl.ds(c, tn)] = (o * conv).astype(BF)
            return 0

        lax.fori_loop(0, (both // seq) * (wch // tn), unit, 0)

    def norm(base_ref, terms, gain_ref, dest_ref, start, count):
        tm = 32

        def unit(i, _):
            m = pl.multiple_of(start + i * tm, tm)
            parts = []
            for b in range(n):
                part = (
                    residual_scale
                    * base_ref[pl.ds(m, tm), pl.ds(b * nc, nc)].astype(F32)
                    + own[b, pl.ds(m, tm)]
                )
                for term in terms:
                    part = part + term[b, pl.ds(m, tm)].astype(F32)
                parts.append(part)
            total = parts[0]
            for b in range(1, n):
                total = total + parts[b]
            mean = jnp.sum(total, axis=-1, keepdims=True) / d
            parts = [p - mean for p in parts]
            square = parts[0] * parts[0]
            for b in range(1, n):
                square = square + parts[b] * parts[b]
            spread = jnp.sum(square, axis=-1, keepdims=True) / d
            scale = lax.rsqrt(spread + norm_epsilon)
            for b in range(n):
                cols = pl.ds(b * nc, nc)
                dest_ref[pl.ds(m, tm), cols] = (
                    parts[b] * scale * gain_ref[:, cols]
                ).astype(BF)
            return 0

        lax.fori_loop(0, count // tm, unit, 0)

    def near_first(p):
        return mate_copy(
            first_sem + p, fst.at[pl.ds(p * pr, pr)], fst.at[pl.ds(MATE + p * pr, pr)]
        )

    def twin_first(p):
        return across_copy(
            p, fst.at[pl.ds(p * pr, pr)], fst.at[pl.ds(TWIN + p * pr, pr)]
        )

    def diag_first(p):
        return mate_copy(
            diag_sem + p,
            fst.at[pl.ds(TWIN + p * pr, pr)],
            fst.at[pl.ds(DIAG + p * pr, pr)],
        )

    def make_first():
        for k, o in every:
            mix_block(k, o).wait_recv()
        for p in range(pieces):
            norm(tok, (precv1,), norm1_ref, fst, p * pr, pr)
            twin_first(p).start()
            near_first(p).start()

    def take_near():
        for p in range(pieces):
            near_first(p).wait_recv()

    def relay_first(p):
        twin_first(p).wait_recv()
        diag_first(p).start()

    def take_far(p, count):
        for q in range(p, p + count):
            diag_first(q).wait_recv()

    def free_sends():
        for k, o in every:
            mix_block(k, o).wait_send()

    plan = {}

    def after(ti, h, which, *work):
        plan.setdefault((ti, h, which), []).extend(work)

    def project_at(h):
        def work():
            if h:
                arrived(0, h)
            project(h)

        return work

    def mixout_at(h):
        def work():
            if h:
                arrived(1, h)
            mixout(h)

        return work

    def do(function, *values):
        return lambda: function(*values)

    last = half - 1
    until = list(range(half))
    most = pieces - 1
    after(0, 1, 0, project_at(0))
    for h in range(1, last):
        after(0, h + 1, 1, project_at(h))
    after(1, 1, 0, do(arrived, 0, last), do(project, last, (0,)))
    after(1, 1, 1, do(project, last, (1,)))
    after(1, 2, 0, do(project, last, (2,)))
    after(1, 2, 1, project_at(half))
    after(1, last, 0, mix)
    for h in range(half + 1):
        after(1, *((last, 1) if h < last - 1 else (half, 0)), mixout_at(h))
    after(1, half, 0, make_first)
    after(2, 1, 0, take_near, do(raise_near, 0))
    for h in range(1, half):
        after(2, h, 1, do(raise_near, h))
    after(2, 2, 0, do(relay_first, 0))
    after(2, 2, 1, do(relay_first, 1))
    for p in range(2, most):
        after(2, last, 1, do(relay_first, p))
    after(2, last, 1, do(take_far, 0, most), do(raise_far, 0, most, until))
    after(2, half, 0, do(relay_first, most))
    after(2, half, 0, do(raise_far, 0, most, [half]), do(take_far, most, 1))
    after(2, half, 0, do(raise_far, most, 1, until + [half]))
    after(2, half, 0, do(lower_far, 0), do(raise_near, half), do(pass_across, 0))
    after(3, 1, 0, free_sends)
    for h in range(1, half):
        after(3, h, 1, do(lower_far, h), do(lower_near, h - 1), do(pass_across, h))
    after(3, half, 0, do(lower_far, half), do(lower_near, half - 1))
    after(3, half, 0, do(pass_across, half), do(lower_near, half))

    for ti in range(4):
        for e in events(ti):
            event(*e)
            for work in plan.get(e, ()):
                work()

    for k, o in every:
        near_block(k, o).wait_recv()
    for k, o in every:
        across_block(k, o).wait_recv()
    norm(fst, (precv2, xrecv), norm2_ref, out_ref, 0, rows)

    for k, o in every:
        near_block(k, o).wait_send()
        far_block(k, o).wait_send()
        across_block(k, o).wait_send()
    for p in range(pieces):
        near_first(p).wait_send()
        twin_first(p).wait_send()
        diag_first(p).wait_send()
    share.wait_send()
    for key in copies:
        copies[key].wait_send()


def fits(mesh, args):
    n = mesh.shape["fs"]
    rows, d = args[0].shape
    ks, wch = args[1].shape
    nc = args[5].shape[1]
    ff = args[7].shape[1] // 2
    return (
        mesh.shape["rep"] == 2
        and mesh.shape["tp"] == 2
        and n % 2 == 0
        and n >= 8
        and ks % 128 == 0
        and nc == 256
        and wch % 256 == 0
        and ff % 256 == 0
        and wch // 256 <= n
        and wch <= 2 * rows
        and ff <= 4 * rows
        and ks <= rows
        and rows % SEQ == 0
        and rows % 128 == 0
    )


def fused(mesh, *args):
    (
        tokens,
        outer_weight,
        inner_weight,
        value_weight,
        conv_taps,
        mix_out,
        norm_first,
        up_weight,
        down_weight,
        norm_second,
    ) = args
    n = mesh.shape["fs"]
    rows, d = tokens.shape
    ks, wch = outer_weight.shape
    ff = up_weight.shape[1] // 2
    nc = mix_out.shape[1]
    both = 2 * rows
    anywhere = pl.BlockSpec(memory_space=pl.ANY)
    vmem = pl.BlockSpec(memory_space=pltpu.VMEM)
    messages = 4 * (3 * n - 3)
    pairs = 9 + 3 * n
    return pl.pallas_call(
        functools.partial(layer_kernel, n),
        out_shape=jax.ShapeDtypeStruct((rows, d), BF),
        in_specs=[
            anywhere,
            anywhere,
            anywhere,
            anywhere,
            vmem,
            anywhere,
            vmem,
            anywhere,
            anywhere,
            vmem,
        ],
        out_specs=vmem,
        scratch_shapes=[
            pltpu.VMEM((3, n, ks, wch), BF),
            pltpu.VMEM((n, wch, nc), BF),
            pltpu.VMEM((n * ks, ff), BF),
            pltpu.VMEM((n, ff, nc), BF),
            pltpu.VMEM((both, d), BF),
            pltpu.VMEM((2 * both, max(wch, ff)), F32),
            pltpu.VMEM((both, wch), BF),
            pltpu.VMEM((n, both, nc), F32),
            pltpu.VMEM((n, both, nc), BF),
            pltpu.VMEM((n, rows, nc), BF),
            pltpu.VMEM((n, both, nc), BF),
            pltpu.VMEM((n, rows, nc), BF),
            pltpu.VMEM((n, rows, nc), BF),
            pltpu.VMEM((2 * both, d), BF),
            pltpu.VMEM((2 * both, ff), BF),
            pltpu.SemaphoreType.DMA((8,)),
            pltpu.SemaphoreType.DMA((messages,)),
            pltpu.SemaphoreType.DMA((messages,)),
            pltpu.SemaphoreType.DMA((pairs,)),
            pltpu.SemaphoreType.DMA((pairs,)),
            pltpu.SemaphoreType.DMA((4 + n,)),
            pltpu.SemaphoreType.DMA((4 + n,)),
        ],
        compiler_params=pltpu.CompilerParams(
            collective_id=0, has_side_effects=True, vmem_limit_bytes=67043328
        ),
        name="layer",
    )(
        tokens,
        outer_weight,
        inner_weight,
        value_weight,
        conv_taps,
        mix_out,
        norm_first.reshape(1, d),
        up_weight,
        down_weight,
        norm_second.reshape(1, d),
    )


def solution(mesh):
    def body(*args):
        return fused(mesh, *args) if fits(mesh, args) else local(*args)

    return jax.shard_map(
        body,
        mesh=mesh,
        in_specs=(
            P(("rep", "fs", "tp"), None),
            P("fs", "tp"),
            P("fs", "tp"),
            P("fs", "tp"),
            P(None, "tp"),
            P("tp", "fs"),
            P(),
            P("fs", "tp"),
            P("tp", "fs"),
            P(),
        ),
        out_specs=P(("rep", "fs", "tp"), None),
        check_vma=False,
    )
```

profile of v0, /device:TPU:0, one launch (start us, length us, event | category | flops | bytes accessed | tf_op | source)
XLA Modules:
  0.0 190.3 jit_solution(3297199018411436793)
XLA Ops:
  0.0 187.6 %layer.1 = bf16[384,2048]{1,0:T(8,128)(2,1)} custom-call(bf16[384,2048]{1,0:T(8,128)(2,1)} %tokens_hbm.1, f32[256,768]{1,0:T(8,128)} %outer_hbm.1, f32[256,768]{1,0:T(8,128)} %inner_hbm.1, f32[256,768]{1,0:T(8,128)} %value_hbm.1, f32[3,768]{1,0:T(4,128)} %taps_ref.1, f32[768,256]{1,0:T(8,128)} %mix_hbm.1, f32[1,2048]{1,0:T(1,128)} %bitcast.2, ...), custom_call_target="tpu_custom_call" | custom-call | tf_op jit(solution)/shard_map/layer/pallas_call | solution.py:688
  187.6 2.7 %copy.12 = bf16[384,2048]{1,0:T(8,128)(2,1)} copy(bf16[384,2048]{1,0:T(8,128)(2,1)} %layer.1) | data formatting | bytes 3145728
where the time goes:
time: 191 us; the launch traced here: 190 us
  Pallas kernels  188 us (98%)
  local copies, waits for them, and re-layouts  2.73 us (1%)
    pallas_call x1, Pallas kernels, fused(): pl.pallas_call(functools.partial(layer_kernel, n), out_shape=jax.ShapeDty...  188 us

commit v1 on v0

v1 whole, which is shorter than its diff:
```python
import functools

import jax
import jax.numpy as jnp
from jax import lax
from jax.experimental import pallas as pl
from jax.experimental.pallas import tpu as pltpu
from jax.sharding import PartitionSpec as P

SEQ = 128


residual_scale = 2.0**0.25
norm_epsilon = 1e-05


def layer_norm(values, scaling):
    center = values - jnp.mean(values, axis=-1, keepdims=True)
    spread = jnp.mean(center * center, axis=-1, keepdims=True)
    return center * lax.rsqrt(spread + norm_epsilon) * scaling


def short_conv(product, conv_taps):
    places = jnp.arange(product.shape[0], dtype=jnp.int32) % SEQ
    blank = jnp.zeros((1, product.shape[1]), jnp.float32)
    before = jnp.concatenate([blank, product[:-1]], axis=0)
    after = jnp.concatenate([product[1:], blank], axis=0)
    before = jnp.where((places > 0)[:, None], before, 0.0)
    after = jnp.where((places < SEQ - 1)[:, None], after, 0.0)
    return conv_taps[0] * before + conv_taps[1] * product + conv_taps[2] * after


def local(
    tokens,
    outer_weight,
    inner_weight,
    value_weight,
    conv_taps,
    mix_out,
    norm_first,
    up_weight,
    down_weight,
    norm_second,
):
    grouped = lax.all_gather(tokens, "tp", axis=0, tiled=True)
    outer_bf = outer_weight.astype(jnp.bfloat16)
    inner_bf = inner_weight.astype(jnp.bfloat16)
    value_bf = value_weight.astype(jnp.bfloat16)
    outer_full, inner_full, value_full = (
        lax.all_gather(outer_bf, "fs", axis=0, tiled=True),
        lax.all_gather(inner_bf, "fs", axis=0, tiled=True),
        lax.all_gather(value_bf, "fs", axis=0, tiled=True),
    )
    outer = jnp.dot(grouped, outer_full, preferred_element_type=jnp.float32)
    inner = jnp.dot(grouped, inner_full, preferred_element_type=jnp.float32)
    value = jnp.dot(grouped, value_full, preferred_element_type=jnp.float32)
    mixed = (outer * short_conv(inner * value, conv_taps)).astype(jnp.bfloat16)
    mixout_full = lax.all_gather(mix_out.astype(jnp.bfloat16), "fs", axis=1, tiled=True)
    selected = mixed
    mixing = lax.psum_scatter(
        jnp.dot(selected, mixout_full, preferred_element_type=jnp.float32).astype(jnp.bfloat16),
        "tp",
        scatter_dimension=0,
        tiled=True,
    ).astype(jnp.float32)
    first = layer_norm(residual_scale * tokens.astype(jnp.float32) + mixing, norm_first).astype(
        jnp.bfloat16
    )
    grouped_first = lax.all_gather(first, "tp", axis=0, tiled=True)
    upward_bf = up_weight.astype(jnp.bfloat16)
    upward_full = lax.all_gather(upward_bf, "fs", axis=0, tiled=True)
    raised = jnp.dot(grouped_first, upward_full, preferred_element_type=jnp.float32)
    raised = jax.nn.relu(raised)
    hidden = (raised * raised).astype(jnp.bfloat16)
    down_full = lax.all_gather(down_weight.astype(jnp.bfloat16), "fs", axis=1, tiled=True)
    selected = hidden
    lowered = lax.psum_scatter(
        jnp.dot(selected, down_full, preferred_element_type=jnp.float32).astype(jnp.bfloat16),
        "tp",
        scatter_dimension=0,
        tiled=True,
    ).astype(jnp.float32)
    return layer_norm(residual_scale * first.astype(jnp.float32) + lowered, norm_second).astype(
        jnp.bfloat16
    )


MESH = pl.DeviceIdType.MESH
BF = jnp.bfloat16
F32 = jnp.float32


def dot(a, b):
    return jnp.dot(a, b, preferred_element_type=F32)


def layer_kernel(
    n,
    tokens_hbm,
    outer_hbm,
    inner_hbm,
    value_hbm,
    taps_ref,
    mix_hbm,
    norm1_ref,
    up_hbm,
    down_hbm,
    norm2_ref,
    out_ref,
    wa,
    wb,
    wc,
    wd,
    tok,
    acc,
    mixed,
    own,
    psend,
    precv,
    xsend,
    xrecv,
    fst,
    hid,
    load_sem,
    ring_send,
    ring_recv,
    tp_send,
    tp_recv,
    x_send,
    x_recv,
):
    half = n // 2
    r = lax.axis_index("rep")
    f = lax.axis_index("fs")
    t = lax.axis_index("tp")
    rows = tokens_hbm.shape[0]
    both = 2 * rows
    d = tokens_hbm.shape[1]
    ks = outer_hbm.shape[0]
    wch = wb.shape[1]
    ff = wc.shape[1]
    nc = wb.shape[2]
    OWN, TWIN, MATE, DIAG = 0, rows, 2 * rows, 3 * rows

    odd = f % 2
    pos = (1 - odd) * (f // 2) + odd * (n - 1 - f // 2)

    def at(place):
        p = (place + 2 * n) % n
        hi = p // half
        return (1 - hi) * (2 * p) + hi * (2 * (n - 1 - p) + 1)

    right = {"fs": at(pos + 1)}
    left = {"fs": at(pos - 1)}
    across = {"rep": 1 - r}
    mate = {"tp": 1 - t}

    def owners(h):
        if h == 0:
            return [f]
        if h == half:
            return [at(pos + half)]
        return [at(pos - h), at(pos + h)]

    def numbered(h):
        return [(0 if h == 0 else 2 * h - 1 + k, o) for k, o in enumerate(owners(h))]

    every = [item for h in range(half + 1) for item in numbered(h)]

    mine = pl.multiple_of(r * ff, 128)
    share_at = pl.multiple_of(r * wch, 128)
    first_down = min(ff, both)
    rest_down = ff - first_down
    loads = [
        pltpu.make_async_copy(
            src.at[:, pl.ds(share_at, wch)],
            acc.at[pl.ds(i * ks, ks), pl.ds(0, wch)],
            load_sem.at[i],
        )
        for i, src in enumerate((outer_hbm, inner_hbm, value_hbm))
    ]
    loads += [
        pltpu.make_async_copy(
            mix_hbm.at[pl.ds(share_at, wch)], own.at[0, pl.ds(0, wch)], load_sem.at[3]
        ),
        pltpu.make_async_copy(
            up_hbm.at[:, pl.ds(mine, ff)],
            acc.at[pl.ds(3 * ks, ks), pl.ds(0, ff)],
            load_sem.at[4],
        ),
        pltpu.make_async_copy(
            down_hbm.at[pl.ds(mine, first_down)],
            own.at[1, pl.ds(0, first_down)],
            load_sem.at[5],
        ),
        pltpu.make_async_copy(tokens_hbm, tok.at[pl.ds(0, rows)], load_sem.at[6]),
    ]
    if rest_down:
        loads.append(
            pltpu.make_async_copy(
                down_hbm.at[pl.ds(mine + first_down, rest_down)],
                own.at[2, pl.ds(0, rest_down)],
                load_sem.at[7],
            )
        )
    for load in loads[:3]:
        load.start()

    barrier = pltpu.get_barrier_semaphore()
    for device in (right, left, across, mate):
        pl.semaphore_signal(barrier, inc=1, device_id=device, device_id_type=MESH)
    pl.semaphore_wait(barrier, 4)

    mate_copies = {}
    across_copies = {}

    def mate_copy(key, src, dst):
        if key not in mate_copies:
            i = len(mate_copies)
            mate_copies[key] = pltpu.make_async_remote_copy(
                src_ref=src,
                dst_ref=dst,
                send_sem=tp_send.at[i],
                recv_sem=tp_recv.at[i],
                device_id=mate,
                device_id_type=MESH,
            )
        return mate_copies[key]

    def across_copy(key, src, dst):
        if key not in across_copies:
            i = len(across_copies)
            across_copies[key] = pltpu.make_async_remote_copy(
                src_ref=src,
                dst_ref=dst,
                send_sem=x_send.at[i],
                recv_sem=x_recv.at[i],
                device_id=across,
                device_id_type=MESH,
            )
        return across_copies[key]

    def piece(ti, which, owner):
        if ti == 0:
            u = ks // 2
            return wa.at[pl.ds(pl.multiple_of(owner * ks + which * u, 16), u)]
        if ti == 1:
            return wb.at[owner, pl.ds(which * (wch // 2), wch // 2)]
        if ti == 2:
            u = ks // 2
            return wc.at[pl.ds(pl.multiple_of(owner * ks + which * u, 16), u)]
        return wd.at[owner, pl.ds(which * (ff // 2), ff // 2)]

    per = 4 * half - 2
    index = {}
    for h in range(1, half + 1):
        for kind in ("Rq", "Rp", "Lq", "Lp"):
            if h == half and kind in ("Rp", "Lq"):
                continue
            index[kind, h] = len(index)

    copies = {}

    def message(ti, kind, h):
        key = (ti, kind, h)
        if key not in copies:
            which = int(kind[1] == "p")
            if kind[0] == "R":
                src, device = at(pos - (h - 1)), right
            else:
                src, device = at(pos + (h - 1)), left
            i = ti * per + index[kind, h]
            ref = piece(ti, which, src)
            copies[key] = pltpu.make_async_remote_copy(
                src_ref=ref,
                dst_ref=ref,
                send_sem=ring_send.at[i],
                recv_sem=ring_recv.at[i],
                device_id=device,
                device_id_type=MESH,
            )
        return copies[key]

    def send(ti, kind, h):
        if ti < 4 and (kind, h) in index:
            message(ti, kind, h).start()

    def got(ti, kind, h):
        message(ti, kind, h).wait_recv()

    def event(ti, h, which):
        if which == 0:
            got(ti, "Rq", h)
            send(ti, "Rq", h + 1)
            if h == half:
                send(ti + 1, "Rp", 1)
            got(ti, "Lp", h)
            send(ti, "Lp", h + 1)
            if h == half:
                send(ti + 1, "Lq", 1)
        else:
            got(ti, "Rp", h)
            if h + 1 < half:
                send(ti, "Rp", h + 1)
            else:
                send(ti + 1, "Rq", 1)
            got(ti, "Lq", h)
            if h + 1 < half:
                send(ti, "Lq", h + 1)
            else:
                send(ti + 1, "Lp", 1)

    def events(ti):
        out = []
        for h in range(1, half + 1):
            out.append((ti, h, 0))
            if h < half:
                out.append((ti, h, 1))
        return out

    def block_of(o):
        return pl.ds(pl.multiple_of(o * ks, 128), ks)

    def twin_tokens(k, o):
        return across_copy(
            ("tok", k),
            tokens_hbm.at[:, block_of(o)],
            tok.at[pl.ds(TWIN, rows), block_of(o)],
        )

    def diag_tokens(k, o):
        return mate_copy(
            ("tok", k),
            tok.at[pl.ds(TWIN, rows), block_of(o)],
            tok.at[pl.ds(DIAG, rows), block_of(o)],
        )

    share = mate_copy("share", tokens_hbm, tok.at[pl.ds(MATE, rows)])
    for k, o in every:
        twin_tokens(k, o).start()
    for i in range(3):
        loads[i].wait()
        wa[pl.ds(pl.multiple_of(f * ks, 16), ks), pl.ds(i * wch, wch)] = acc[
            pl.ds(i * ks, ks), pl.ds(0, wch)
        ].astype(BF)
    send(0, "Rq", 1)
    send(0, "Lp", 1)
    send(0, "Rp", 1)
    send(0, "Lq", 1)
    for load in loads[3:]:
        load.start()
    share.start()
    loads[3].wait()
    wb[f] = own[0, pl.ds(0, wch)].astype(BF)
    loads[4].wait()
    wc[pl.ds(pl.multiple_of(f * ks, 16), ks), :] = acc[
        pl.ds(3 * ks, ks), pl.ds(0, ff)
    ].astype(BF)
    loads[5].wait()
    wd[f, pl.ds(0, first_down)] = own[1, pl.ds(0, first_down)].astype(BF)
    if rest_down:
        loads[7].wait()
        wd[f, pl.ds(first_down, rest_down)] = own[2, pl.ds(0, rest_down)].astype(BF)
    loads[6].wait()
    share.wait_recv()

    tn = 256
    seq = SEQ
    pieces = rows // seq
    most = pieces - 1
    EARLY, LATE, ALL = (0, most * seq), (most * seq, seq), (0, rows)

    def relay_tokens(h):
        for k, o in numbered(h):
            twin_tokens(k, o).wait_recv()
            diag_tokens(k, o).start()

    def project(h, base):
        who = owners(h)

        def unit(i, _):
            m = pl.ds(pl.multiple_of(i % 2 * MATE + base, 16), rows)
            c = pl.ds(pl.multiple_of(i // 2 * wch, 128), wch)
            total = None
            for o in who:
                w = wa[pl.ds(pl.multiple_of(o * ks, 16), ks), c]
                term = dot(tok[m, block_of(o)], w)
                total = term if total is None else total + term
            if h == 0:
                acc[m, c] = total
            else:
                acc[m, c] += total
            return 0

        lax.fori_loop(0, 2 * 3, unit, 0)

    def project_near(h):
        project(h, OWN)

    def project_far(h):
        for k, o in numbered(h):
            diag_tokens(k, o).wait_recv()
        project(h, TWIN)

    def mix(base, part):
        start, count = part
        tc = 128
        seqs = count // seq

        def unit(i, _):
            j = i % (2 * seqs)
            m = pl.ds(
                pl.multiple_of(base + j // seqs * MATE + start + j % seqs * seq, seq), seq
            )
            c = pl.multiple_of(i // (2 * seqs) * tc, tc)
            o = acc[m, pl.ds(c, tc)]
            p = (
                acc[m, pl.ds(pl.multiple_of(wch + c, tc), tc)]
                * acc[m, pl.ds(pl.multiple_of(2 * wch + c, tc), tc)]
            )
            place = lax.broadcasted_iota(jnp.int32, p.shape, 0)
            before = jnp.where(place > 0, pltpu.roll(p, 1, 0), 0.0)
            after = jnp.where(place < seq - 1, pltpu.roll(p, seq - 1, 0), 0.0)
            taps = taps_ref[:, pl.ds(pl.multiple_of(share_at + c, tc), tc)]
            conv = taps[0:1] * before + taps[1:2] * p + taps[2:3] * after
            mixed[m, pl.ds(c, tc)] = (o * conv).astype(BF)
            return 0

        lax.fori_loop(0, 2 * seqs * (wch // tc), unit, 0)

    def raise_part(size, start, x_base, acc_base, hs, new, final):
        who = [o for h in hs for o in owners(h)]
        tiles = ff // tn

        def unit(i, _):
            side = i % 2
            c = pl.ds(pl.multiple_of(i // 2 * tn, tn), tn)
            x_row = pl.multiple_of(x_base + side * MATE + start, 16)
            total = None
            for o in who:
                x = fst[pl.ds(x_row, size), block_of(o)]
                term = dot(x, wc[pl.ds(pl.multiple_of(o * ks, 16), ks), c])
                total = term if total is None else total + term
            span = pl.ds(pl.multiple_of(acc_base + side * rows + start, 16), size)
            if not new:
                total = total + acc[span, c]
            if final:
                total = jnp.maximum(total, 0.0)
                hid[pl.ds(x_row, size), c] = (total * total).astype(BF)
            else:
                acc[span, c] = total
            return 0

        lax.fori_loop(0, 2 * tiles, unit, 0)

    def raise_near(h):
        raise_part(rows, 0, OWN, 0, [h], h == 0, h == half)

    def raise_far(part):
        start, count = part
        for p in range(start // seq, (start + count) // seq):
            diag_first(p).wait_recv()
        raise_part(count, start, TWIN, both, range(half + 1), True, True)

    def far_block(kind, k, o, part):
        span = pl.ds(rows + part[0], part[1])
        return mate_copy((kind, k, part), psend.at[o, span], precv.at[o, span])

    def near_block(kind, k, o):
        span = pl.ds(0, rows)
        return mate_copy((kind, k), psend.at[o, span], precv.at[o, span])

    def across_block(kind, k, o, part):
        span = pl.ds(*part)
        return across_copy((kind, k, part), xsend.at[o, span], xrecv.at[o, span])

    used = []

    def far(kind, x_ref, w_ref, h, part):
        start, count = part
        for k, o in numbered(h):
            span = pl.ds(rows + start, count)
            psend[o, span] = dot(x_ref[pl.ds(DIAG + start, count), :], w_ref[o]).astype(BF)
            far_block(kind, k, o, part).start()
            own[o, span] = dot(x_ref[pl.ds(TWIN + start, count), :], w_ref[o])

    def pass_far(kind, h, part):
        start, count = part
        for k, o in numbered(h):
            far_block(kind, k, o, part).wait_recv()
            span = pl.ds(rows + start, count)
            xsend[o, pl.ds(start, count)] = (own[o, span] + precv[o, span].astype(F32)).astype(BF)
            across_block(kind, k, o, part).start()
            used.append((kind, k, o, part))

    def near(kind, x_ref, w_ref, h):
        span = pl.ds(0, rows)
        for k, o in numbered(h):
            psend[o, span] = dot(x_ref[pl.ds(MATE, rows), :], w_ref[o]).astype(BF)
            near_block(kind, k, o).start()
            own[o, span] = dot(x_ref[pl.ds(OWN, rows), :], w_ref[o])

    def mixout_far(h, part):
        far("mix", mixed, wb, h, part)

    def mixout_near(h):
        near("mix", mixed, wb, h)

    def lower_far(h, part):
        far("low", hid, wd, h, part)

    def lower_near(h):
        near("low", hid, wd, h)

    def mix_pass(h, part):
        pass_far("mix", h, part)

    def low_pass(h, part):
        pass_far("low", h, part)

    def norm(base_ref, gain_ref, dest_ref, start, count):
        tm = 32

        def unit(i, _):
            m = pl.multiple_of(start + i * tm, tm)
            parts = []
            for b in range(n):
                part = (
                    residual_scale
                    * base_ref[pl.ds(m, tm), pl.ds(b * nc, nc)].astype(F32)
                    + own[b, pl.ds(m, tm)]
                )
                for term in (precv, xrecv):
                    part = part + term[b, pl.ds(m, tm)].astype(F32)
                parts.append(part)
            total = parts[0]
            for b in range(1, n):
                total = total + parts[b]
            mean = jnp.sum(total, axis=-1, keepdims=True) / d
            parts = [p - mean for p in parts]
            square = parts[0] * parts[0]
            for b in range(1, n):
                square = square + parts[b] * parts[b]
            spread = jnp.sum(square, axis=-1, keepdims=True) / d
            scale = lax.rsqrt(spread + norm_epsilon)
            for b in range(n):
                cols = pl.ds(b * nc, nc)
                dest_ref[pl.ds(m, tm), cols] = (
                    parts[b] * scale * gain_ref[:, cols]
                ).astype(BF)
            return 0

        lax.fori_loop(0, count // tm, unit, 0)

    def near_first(p):
        return mate_copy(
            ("near", p), fst.at[pl.ds(p * seq, seq)], fst.at[pl.ds(MATE + p * seq, seq)]
        )

    def twin_first(p):
        return across_copy(
            ("twin", p), fst.at[pl.ds(p * seq, seq)], fst.at[pl.ds(TWIN + p * seq, seq)]
        )

    def diag_first(p):
        return mate_copy(
            ("diag", p),
            fst.at[pl.ds(TWIN + p * seq, seq)],
            fst.at[pl.ds(DIAG + p * seq, seq)],
        )

    def take_near_sums(kind):
        for k, o in every:
            near_block(kind, k, o).wait_recv()

    def make_first(part):
        for k, o in every:
            across_block("mix", k, o, part).wait_recv()
        start, count = part
        for p in range(start // seq, (start + count) // seq):
            norm(tok, norm1_ref, fst, p * seq, seq)
            twin_first(p).start()
            near_first(p).start()

    def take_near():
        for p in range(pieces):
            near_first(p).wait_recv()

    def relay_first(p):
        twin_first(p).wait_recv()
        diag_first(p).start()

    def free_sends():
        for k, o in every:
            near_block("mix", k, o).wait_send()
            for part in (EARLY, LATE):
                far_block("mix", k, o, part).wait_send()
                across_block("mix", k, o, part).wait_send()

    plan = {}

    def after(ti, h, which, *work):
        plan.setdefault((ti, h, which), []).extend(work)

    def do(function, *values):
        return lambda: function(*values)

    last = half - 1

    after(0, 1, 0, do(relay_tokens, 0), do(project_near, 0), do(project_far, 0))
    for h in range(1, last):
        after(0, h, 1, do(relay_tokens, h))
        after(0, h + 1, 0, do(project_near, h), do(project_far, h))
    after(0, last, 1, do(relay_tokens, last), do(relay_tokens, half))
    after(0, last, 1, do(project_near, last), do(project_far, last))
    after(0, half, 0, do(project_far, half), do(mix, TWIN, EARLY), do(mixout_far, 0, EARLY))
    after(1, 1, 0, do(project_near, half), do(mix_pass, 0, EARLY), do(mix, TWIN, LATE))
    after(1, 1, 1, do(mixout_far, 1, EARLY), do(mix, OWN, ALL))
    after(1, 2, 0, do(mix_pass, 1, EARLY))
    for h in range(2, half):
        after(1, h, 1, do(mixout_far, h, EARLY))
        after(1, h + 1, 0, do(mix_pass, h, EARLY))
    after(1, half, 0, do(mixout_far, half, EARLY), do(mixout_far, 0, LATE))
    after(1, half, 0, do(mix_pass, half, EARLY))
    for h in range(1, half + 1):
        after(1, half, 0, do(mixout_far, h, LATE), do(mix_pass, h - 1, LATE))
    after(1, half, 0, do(mix_pass, half, LATE))
    for h in range(half + 1):
        after(1, half, 0, do(mixout_near, h))
    after(2, 1, 1, do(take_near_sums, "mix"), do(make_first, EARLY))
    after(2, 2, 1, do(make_first, LATE), do(take_near))
    after(2, 2, 1, do(raise_near, 0), do(raise_near, 1))
    after(2, 3, 0, do(raise_near, 2), do(free_sends))
    for h in range(3, half):
        after(2, h, 1, do(raise_near, h))
    after(2, half, 0, do(relay_first, 0), do(raise_near, half))
    for p in range(1, most):
        after(3, 1, 1, do(relay_first, p))
    after(3, 1, 1, do(lower_near, 0), do(raise_far, EARLY), do(lower_far, 0, EARLY))
    after(3, 1, 1, do(lower_far, 1, EARLY), do(low_pass, 0, EARLY))
    after(3, 2, 0, do(low_pass, 1, EARLY), do(lower_near, 1))
    after(3, 2, 0, do(relay_first, most), do(raise_far, LATE))
    after(3, 2, 0, do(lower_far, 0, LATE), do(lower_far, 1, LATE))
    after(3, 2, 0, do(low_pass, 0, LATE), do(low_pass, 1, LATE))
    for h in range(2, half):
        after(3, h, 1, do(lower_far, h, ALL), do(lower_near, h), do(low_pass, h, ALL))
    after(3, half, 0, do(lower_far, half, ALL), do(lower_near, half))
    after(3, half, 0, do(low_pass, half, ALL))

    for ti in range(4):
        for e in events(ti):
            event(*e)
            for work in plan.get(e, ()):
                work()

    take_near_sums("low")
    for kind, k, o, part in used:
        if kind == "low":
            across_block(kind, k, o, part).wait_recv()
    norm(fst, norm2_ref, out_ref, 0, rows)

    for key, copy in mate_copies.items():
        if key[0] != "mix":
            copy.wait_send()
    for key, copy in across_copies.items():
        if key[0] != "mix":
            copy.wait_send()
    for key in copies:
        copies[key].wait_send()


def fits(mesh, args):
    n = mesh.shape["fs"]
    rows, d = args[0].shape
    ks = args[1].shape[0]
    wch = args[1].shape[1] // 2
    nc = args[5].shape[1]
    ff = args[7].shape[1] // 2
    return (
        mesh.shape["rep"] == 2
        and mesh.shape["tp"] == 2
        and n % 2 == 0
        and n >= 8
        and ks % 128 == 0
        and nc == 256
        and wch % 128 == 0
        and ff % 256 == 0
        and wch <= 2 * rows
        and ff <= 4 * rows
        and ff <= 3 * wch
        and ks <= rows
        and rows % SEQ == 0
        and rows >= 2 * SEQ
    )


def fused(mesh, *args):
    (
        tokens,
        outer_weight,
        inner_weight,
        value_weight,
        conv_taps,
        mix_out,
        norm_first,
        up_weight,
        down_weight,
        norm_second,
    ) = args
    n = mesh.shape["fs"]
    rows, d = tokens.shape
    ks = outer_weight.shape[0]
    wch = outer_weight.shape[1] // 2
    ff = up_weight.shape[1] // 2
    nc = mix_out.shape[1]
    both = 2 * rows
    anywhere = pl.BlockSpec(memory_space=pl.ANY)
    vmem = pl.BlockSpec(memory_space=pltpu.VMEM)
    messages = 4 * (2 * n - 2)
    pairs = 1 + n + 6 * n + 2 * (rows // SEQ)
    crosses = n + 4 * n + rows // SEQ
    return pl.pallas_call(
        functools.partial(layer_kernel, n),
        out_shape=jax.ShapeDtypeStruct((rows, d), BF),
        in_specs=[
            anywhere,
            anywhere,
            anywhere,
            anywhere,
            vmem,
            anywhere,
            vmem,
            anywhere,
            anywhere,
            vmem,
        ],
        out_specs=vmem,
        scratch_shapes=[
            pltpu.VMEM((n * ks, 3 * wch), BF),
            pltpu.VMEM((n, wch, nc), BF),
            pltpu.VMEM((n * ks, ff), BF),
            pltpu.VMEM((n, ff, nc), BF),
            pltpu.VMEM((2 * both, d), BF),
            pltpu.VMEM((2 * both, 3 * wch), F32),
            pltpu.VMEM((2 * both, wch), BF),
            pltpu.VMEM((n, both, nc), F32),
            pltpu.VMEM((n, both, nc), BF),
            pltpu.VMEM((n, both, nc), BF),
            pltpu.VMEM((n, rows, nc), BF),
            pltpu.VMEM((n, rows, nc), BF),
            pltpu.VMEM((2 * both, d), BF),
            pltpu.VMEM((2 * both, ff), BF),
            pltpu.SemaphoreType.DMA((8,)),
            pltpu.SemaphoreType.DMA((messages,)),
            pltpu.SemaphoreType.DMA((messages,)),
            pltpu.SemaphoreType.DMA((pairs,)),
            pltpu.SemaphoreType.DMA((pairs,)),
            pltpu.SemaphoreType.DMA((crosses,)),
            pltpu.SemaphoreType.DMA((crosses,)),
        ],
        compiler_params=pltpu.CompilerParams(
            collective_id=0, has_side_effects=True, vmem_limit_bytes=67043328
        ),
        name="layer",
    )(
        tokens,
        outer_weight,
        inner_weight,
        value_weight,
        conv_taps,
        mix_out,
        norm_first.reshape(1, d),
        up_weight,
        down_weight,
        norm_second.reshape(1, d),
    )


def solution(mesh):
    def body(*args):
        return fused(mesh, *args) if fits(mesh, args) else local(*args)

    return jax.shard_map(
        body,
        mesh=mesh,
        in_specs=(
            P(("rep", "fs", "tp"), None),
            P("fs", "tp"),
            P("fs", "tp"),
            P("fs", "tp"),
            P(None, "tp"),
            P("tp", "fs"),
            P(),
            P("fs", "tp"),
            P("tp", "fs"),
            P(),
        ),
        out_specs=P(("rep", "fs", "tp"), None),
        check_vma=False,
    )
```

time: 191 us -> 172 us (0.901)
  Pallas kernels: 188 us -> 169 us
    pallas_call x1, Pallas kernels: 188 us -> 169 us  [fused(): pl.pallas_call(functools.partial(layer_kernel, n), out_shape=jax.ShapeDty...]
where the time goes in v1:
time: 172 us
  Pallas kernels  169 us (98%)
  local copies, waits for them, and re-layouts  2.73 us (2%)
    pallas_call x1, Pallas kernels, fused(): pl.pallas_call(functools.partial(layer_kernel, n), out_shape=jax.ShapeDty...  169 us

profile of v1, /device:TPU:0, one launch (start us, length us, event | category | flops | bytes accessed | tf_op | source)
XLA Modules:
  0.0 172.1 jit_solution(8150318080178289306)
XLA Ops:
  0.0 169.3 %layer.1 = bf16[384,2048]{1,0:T(8,128)(2,1)} custom-call(bf16[384,2048]{1,0:T(8,128)(2,1)} %tokens_hbm.1, f32[256,768]{1,0:T(8,128)} %outer_hbm.1, f32[256,768]{1,0:T(8,128)} %inner_hbm.1, f32[256,768]{1,0:T(8,128)} %value_hbm.1, f32[3,768]{1,0:T(4,128)} %taps_ref.1, f32[768,256]{1,0:T(8,128)} %mix_hbm.1, f32[1,2048]{1,0:T(1,128)} %bitcast.2, ...), custom_call_target="tpu_custom_call" | custom-call | tf_op jit(solution)/shard_map/layer/pallas_call | solution.py:722
  169.3 2.7 %copy.12 = bf16[384,2048]{1,0:T(8,128)(2,1)} copy(bf16[384,2048]{1,0:T(8,128)(2,1)} %layer.1) | data formatting | bytes 3145728

commit v2 on v1

--- a/solution.py
+++ b/solution.py
@@ -121,6 +121,7 @@
     xrecv,
     fst,
     hid,
+    stage,
     load_sem,
     ring_send,
     ring_recv,
@@ -375,11 +376,12 @@
             twin_tokens(k, o).wait_recv()
             diag_tokens(k, o).start()
 
-    def project(h, base):
+    def project(h, base, part):
         who = owners(h)
+        start, count = part
 
         def unit(i, _):
-            m = pl.ds(pl.multiple_of(i % 2 * MATE + base, 16), rows)
+            m = pl.ds(pl.multiple_of(i % 2 * MATE + base + start, 16), count)
             c = pl.ds(pl.multiple_of(i // 2 * wch, 128), wch)
             total = None
             for o in who:
@@ -395,12 +397,13 @@
         lax.fori_loop(0, 2 * 3, unit, 0)
 
     def project_near(h):
-        project(h, OWN)
-
-    def project_far(h):
-        for k, o in numbered(h):
-            diag_tokens(k, o).wait_recv()
-        project(h, TWIN)
+        project(h, OWN, ALL)
+
+    def project_far(h, part):
+        if part[0] == 0:
+            for k, o in numbered(h):
+                diag_tokens(k, o).wait_recv()
+        project(h, TWIN, part)
 
     def mix(base, part):
         start, count = part
@@ -607,26 +610,28 @@
 
     last = half - 1
 
-    after(0, 1, 0, do(relay_tokens, 0), do(project_near, 0), do(project_far, 0))
+    after(0, 1, 0, do(relay_tokens, 0), do(project_near, 0), do(project_far, 0, ALL))
     for h in range(1, last):
         after(0, h, 1, do(relay_tokens, h))
-        after(0, h + 1, 0, do(project_near, h), do(project_far, h))
+        after(0, h + 1, 0, do(project_near, h), do(project_far, h, ALL))
     after(0, last, 1, do(relay_tokens, last), do(relay_tokens, half))
-    after(0, last, 1, do(project_near, last), do(project_far, last))
-    after(0, half, 0, do(project_far, half), do(mix, TWIN, EARLY), do(mixout_far, 0, EARLY))
-    after(1, 1, 0, do(project_near, half), do(mix_pass, 0, EARLY), do(mix, TWIN, LATE))
-    after(1, 1, 1, do(mixout_far, 1, EARLY), do(mix, OWN, ALL))
+    after(0, last, 1, do(project_near, last), do(project_far, last, ALL))
+    after(0, half, 0, do(project_far, half, EARLY), do(mix, TWIN, EARLY))
+    after(0, half, 0, do(mixout_far, 0, EARLY))
+    after(1, 1, 0, do(project_far, half, LATE), do(mix_pass, 0, EARLY), do(mix, TWIN, LATE))
+    after(1, 1, 1, do(mixout_far, 1, EARLY))
     after(1, 2, 0, do(mix_pass, 1, EARLY))
-    for h in range(2, half):
+    after(1, 2, 1, do(mixout_far, 2, EARLY))
+    after(1, 3, 0, do(mix_pass, 2, EARLY), do(project_near, half))
+    for h in range(3, half):
         after(1, h, 1, do(mixout_far, h, EARLY))
         after(1, h + 1, 0, do(mix_pass, h, EARLY))
     after(1, half, 0, do(mixout_far, half, EARLY), do(mixout_far, 0, LATE))
     after(1, half, 0, do(mix_pass, half, EARLY))
     for h in range(1, half + 1):
         after(1, half, 0, do(mixout_far, h, LATE), do(mix_pass, h - 1, LATE))
-    after(1, half, 0, do(mix_pass, half, LATE))
-    for h in range(half + 1):
-        after(1, half, 0, do(mixout_near, h))
+    after(1, half, 0, do(mix, OWN, ALL), do(mix_pass, half, LATE))
+    after(2, 1, 0, *[do(mixout_near, h) for h in range(half + 1)])
     after(2, 1, 1, do(take_near_sums, "mix"), do(make_first, EARLY))
     after(2, 2, 1, do(make_first, LATE), do(take_near))
     after(2, 2, 1, do(raise_near, 0), do(raise_near, 1))
@@ -635,17 +640,15 @@
         after(2, h, 1, do(raise_near, h))
     after(2, half, 0, do(relay_first, 0), do(raise_near, half))
     for p in range(1, most):
-        after(3, 1, 1, do(relay_first, p))
-    after(3, 1, 1, do(lower_near, 0), do(raise_far, EARLY), do(lower_far, 0, EARLY))
-    after(3, 1, 1, do(lower_far, 1, EARLY), do(low_pass, 0, EARLY))
-    after(3, 2, 0, do(low_pass, 1, EARLY), do(lower_near, 1))
-    after(3, 2, 0, do(relay_first, most), do(raise_far, LATE))
+        after(3, 1, 0, do(relay_first, p))
+    after(3, 1, 0, do(lower_near, 0), do(raise_far, EARLY))
+    after(3, 1, 1, do(lower_far, 0, EARLY), do(lower_far, 1, EARLY), do(low_pass, 0, EARLY))
+    after(3, 1, 1, do(low_pass, 1, EARLY), do(relay_first, most), do(raise_far, LATE))
     after(3, 2, 0, do(lower_far, 0, LATE), do(lower_far, 1, LATE))
-    after(3, 2, 0, do(low_pass, 0, LATE), do(low_pass, 1, LATE))
+    after(3, 2, 0, do(low_pass, 0, LATE), do(low_pass, 1, LATE), do(lower_near, 1))
     for h in range(2, half):
-        after(3, h, 1, do(lower_far, h, ALL), do(lower_near, h), do(low_pass, h, ALL))
-    after(3, half, 0, do(lower_far, half, ALL), do(lower_near, half))
-    after(3, half, 0, do(low_pass, half, ALL))
+        after(3, h, 1, do(lower_far, h, ALL), do(low_pass, h, ALL), do(lower_near, h))
+    after(3, half, 0, do(lower_far, half, ALL), do(low_pass, half, ALL), do(lower_near, half))
 
     for ti in range(4):
         for e in events(ti):
@@ -657,7 +660,12 @@
     for kind, k, o, part in used:
         if kind == "low":
             across_block(kind, k, o, part).wait_recv()
-    norm(fst, norm2_ref, out_ref, 0, rows)
+    outs = []
+    for p in range(pieces):
+        span = pl.ds(p * seq, seq)
+        norm(fst, norm2_ref, stage, p * seq, seq)
+        outs.append(pltpu.make_async_copy(stage.at[span], out_ref.at[span], load_sem.at[p]))
+        outs[p].start()
 
     for key, copy in mate_copies.items():
         if key[0] != "mix":
@@ -667,6 +675,8 @@
             copy.wait_send()
     for key in copies:
         copies[key].wait_send()
+    for copy in outs:
+        copy.wait()
 
 
 def fits(mesh, args):
@@ -690,7 +700,7 @@
         and ff <= 3 * wch
         and ks <= rows
         and rows % SEQ == 0
-        and rows >= 2 * SEQ
+        and 2 * SEQ <= rows <= 8 * SEQ
     )
 
 
@@ -734,7 +744,7 @@
             anywhere,
             vmem,
         ],
-        out_specs=vmem,
+        out_specs=anywhere,
         scratch_shapes=[
             pltpu.VMEM((n * ks, 3 * wch), BF),
             pltpu.VMEM((n, wch, nc), BF),
@@ -750,6 +760,7 @@
             pltpu.VMEM((n, rows, nc), BF),
             pltpu.VMEM((2 * both, d), BF),
             pltpu.VMEM((2 * both, ff), BF),
+            pltpu.VMEM((rows, d), BF),
             pltpu.SemaphoreType.DMA((8,)),
             pltpu.SemaphoreType.DMA((messages,)),
             pltpu.SemaphoreType.DMA((messages,)),

time: 172 us -> 169 us (0.983)
  Pallas kernels: 169 us -> 166 us
    pallas_call x1, Pallas kernels: 169 us -> 166 us  [fused(): pl.pallas_call(functools.partial(layer_kernel, n), out_shape=jax.ShapeDty...]
where the time goes in v2:
time: 169 us
  Pallas kernels  166 us (98%)
  local copies, waits for them, and re-layouts  2.73 us (2%)
    pallas_call x1, Pallas kernels, fused(): pl.pallas_call(functools.partial(layer_kernel, n), out_shape=jax.ShapeDty...  166 us

profile of v2, /device:TPU:0, one launch (start us, length us, event | category | flops | bytes accessed | tf_op | source)
XLA Modules:
  0.0 168.7 jit_solution(18168206321574313856)
XLA Ops:
  0.0 166.0 %layer.1 = bf16[384,2048]{1,0:T(8,128)(2,1)} custom-call(bf16[384,2048]{1,0:T(8,128)(2,1)} %tokens_hbm.1, f32[256,768]{1,0:T(8,128)} %outer_hbm.1, f32[256,768]{1,0:T(8,128)} %inner_hbm.1, f32[256,768]{1,0:T(8,128)} %value_hbm.1, f32[3,768]{1,0:T(4,128)} %taps_ref.1, f32[768,256]{1,0:T(8,128)} %mix_hbm.1, f32[1,2048]{1,0:T(1,128)} %bitcast.2, ...), custom_call_target="tpu_custom_call" | custom-call | tf_op jit(solution)/shard_map/layer/pallas_call | solution.py:732
  166.0 2.7 %copy.12 = bf16[384,2048]{1,0:T(8,128)(2,1)} copy(bf16[384,2048]{1,0:T(8,128)(2,1)} %layer.1) | data formatting | bytes 3145728

commit v3 on v2

--- a/solution.py
+++ b/solution.py
@@ -121,7 +121,7 @@
     xrecv,
     fst,
     hid,
-    stage,
+    stats,
     load_sem,
     ring_send,
     ring_recv,
@@ -212,34 +212,36 @@
         pl.semaphore_signal(barrier, inc=1, device_id=device, device_id_type=MESH)
     pl.semaphore_wait(barrier, 4)
 
-    mate_copies = {}
-    across_copies = {}
-
-    def mate_copy(key, src, dst):
-        if key not in mate_copies:
-            i = len(mate_copies)
-            mate_copies[key] = pltpu.make_async_remote_copy(
-                src_ref=src,
-                dst_ref=dst,
-                send_sem=tp_send.at[i],
-                recv_sem=tp_recv.at[i],
-                device_id=mate,
+    def copier(device, send_sems, recv_sems):
+        made, arrivals, groups = {}, {}, {}
+
+        def copy(key, src, dst, group, arrival=None):
+            if key not in made:
+                place = arrival or key
+                made[key] = pltpu.make_async_remote_copy(
+                    src_ref=src,
+                    dst_ref=dst,
+                    send_sem=send_sems.at[groups.setdefault(group, len(groups))],
+                    recv_sem=recv_sems.at[arrivals.setdefault(place, len(arrivals))],
+                    device_id=device,
+                    device_id_type=MESH,
+                )
+            return made[key]
+
+        def whole(ref, group, arrival=None):
+            return pltpu.make_async_remote_copy(
+                src_ref=ref,
+                dst_ref=ref,
+                send_sem=send_sems.at[groups.get(group, 0)],
+                recv_sem=recv_sems.at[arrivals.get(arrival, 0)],
+                device_id=device,
                 device_id_type=MESH,
             )
-        return mate_copies[key]
-
-    def across_copy(key, src, dst):
-        if key not in across_copies:
-            i = len(across_copies)
-            across_copies[key] = pltpu.make_async_remote_copy(
-                src_ref=src,
-                dst_ref=dst,
-                send_sem=x_send.at[i],
-                recv_sem=x_recv.at[i],
-                device_id=across,
-                device_id_type=MESH,
-            )
-        return across_copies[key]
+
+        return copy, whole
+
+    mate_copy, mate_whole = copier(mate, tp_send, tp_recv)
+    across_copy, across_whole = copier(across, x_send, x_recv)
 
     def piece(ti, which, owner):
         if ti == 0:
@@ -275,7 +277,7 @@
             copies[key] = pltpu.make_async_remote_copy(
                 src_ref=ref,
                 dst_ref=ref,
-                send_sem=ring_send.at[i],
+                send_sem=ring_send.at[ti],
                 recv_sem=ring_recv.at[i],
                 device_id=device,
                 device_id_type=MESH,
@@ -327,6 +329,7 @@
             ("tok", k),
             tokens_hbm.at[:, block_of(o)],
             tok.at[pl.ds(TWIN, rows), block_of(o)],
+            "tok",
         )
 
     def diag_tokens(k, o):
@@ -334,9 +337,10 @@
             ("tok", k),
             tok.at[pl.ds(TWIN, rows), block_of(o)],
             tok.at[pl.ds(DIAG, rows), block_of(o)],
+            "tok",
         )
 
-    share = mate_copy("share", tokens_hbm, tok.at[pl.ds(MATE, rows)])
+    share = mate_copy("share", tokens_hbm, tok.at[pl.ds(MATE, rows)], "tok")
     for k, o in every:
         twin_tokens(k, o).start()
     for i in range(3):
@@ -376,13 +380,13 @@
             twin_tokens(k, o).wait_recv()
             diag_tokens(k, o).start()
 
-    def project(h, base, part):
+    def project(h, base, part, sides=2):
         who = owners(h)
         start, count = part
 
         def unit(i, _):
-            m = pl.ds(pl.multiple_of(i % 2 * MATE + base + start, 16), count)
-            c = pl.ds(pl.multiple_of(i // 2 * wch, 128), wch)
+            m = pl.ds(pl.multiple_of(i % sides * MATE + base + start, 16), count)
+            c = pl.ds(pl.multiple_of(i // sides * wch, 128), wch)
             total = None
             for o in who:
                 w = wa[pl.ds(pl.multiple_of(o * ks, 16), ks), c]
@@ -394,28 +398,30 @@
                 acc[m, c] += total
             return 0
 
-        lax.fori_loop(0, 2 * 3, unit, 0)
+        lax.fori_loop(0, sides * 3, unit, 0)
 
     def project_near(h):
         project(h, OWN, ALL)
 
-    def project_far(h, part):
-        if part[0] == 0:
-            for k, o in numbered(h):
-                diag_tokens(k, o).wait_recv()
-        project(h, TWIN, part)
-
-    def mix(base, part):
+    def take_diag_tokens(h):
+        for k, o in numbered(h):
+            diag_tokens(k, o).wait_recv()
+
+    def project_far(h):
+        take_diag_tokens(h)
+        project(h, TWIN, ALL)
+
+    def mix(base, part, sides=2):
         start, count = part
         tc = 128
         seqs = count // seq
 
         def unit(i, _):
-            j = i % (2 * seqs)
+            j = i % (sides * seqs)
             m = pl.ds(
                 pl.multiple_of(base + j // seqs * MATE + start + j % seqs * seq, seq), seq
             )
-            c = pl.multiple_of(i // (2 * seqs) * tc, tc)
+            c = pl.multiple_of(i // (sides * seqs) * tc, tc)
             o = acc[m, pl.ds(c, tc)]
             p = (
                 acc[m, pl.ds(pl.multiple_of(wch + c, tc), tc)]
@@ -429,7 +435,7 @@
             mixed[m, pl.ds(c, tc)] = (o * conv).astype(BF)
             return 0
 
-        lax.fori_loop(0, 2 * seqs * (wch // tc), unit, 0)
+        lax.fori_loop(0, sides * seqs * (wch // tc), unit, 0)
 
     def raise_part(size, start, x_base, acc_base, hs, new, final):
         who = [o for h in hs for o in owners(h)]
@@ -467,25 +473,28 @@
 
     def far_block(kind, k, o, part):
         span = pl.ds(rows + part[0], part[1])
-        return mate_copy((kind, k, part), psend.at[o, span], precv.at[o, span])
+        return mate_copy((kind, k, part), psend.at[o, span], precv.at[o, span], kind)
 
     def near_block(kind, k, o):
         span = pl.ds(0, rows)
-        return mate_copy((kind, k), psend.at[o, span], precv.at[o, span])
+        return mate_copy((kind, k), psend.at[o, span], precv.at[o, span], kind, (kind, "near"))
 
     def across_block(kind, k, o, part):
         span = pl.ds(*part)
-        return across_copy((kind, k, part), xsend.at[o, span], xrecv.at[o, span])
-
-    used = []
-
-    def far(kind, x_ref, w_ref, h, part):
+        arrival = ("mix", part) if kind == "mix" else None
+        return across_copy((kind, k, part), xsend.at[o, span], xrecv.at[o, span], kind, arrival)
+
+    lowered = {h: [EARLY, LATE] if h < 2 else [ALL] for h in range(half + 1)}
+
+    def far(kind, x_ref, w_ref, h, part, sides=(DIAG, TWIN)):
         start, count = part
         for k, o in numbered(h):
             span = pl.ds(rows + start, count)
-            psend[o, span] = dot(x_ref[pl.ds(DIAG + start, count), :], w_ref[o]).astype(BF)
-            far_block(kind, k, o, part).start()
-            own[o, span] = dot(x_ref[pl.ds(TWIN + start, count), :], w_ref[o])
+            if DIAG in sides:
+                psend[o, span] = dot(x_ref[pl.ds(DIAG + start, count), :], w_ref[o]).astype(BF)
+                far_block(kind, k, o, part).start()
+            if TWIN in sides:
+                own[o, span] = dot(x_ref[pl.ds(TWIN + start, count), :], w_ref[o])
 
     def pass_far(kind, h, part):
         start, count = part
@@ -494,7 +503,6 @@
             span = pl.ds(rows + start, count)
             xsend[o, pl.ds(start, count)] = (own[o, span] + precv[o, span].astype(F32)).astype(BF)
             across_block(kind, k, o, part).start()
-            used.append((kind, k, o, part))
 
     def near(kind, x_ref, w_ref, h):
         span = pl.ds(0, rows)
@@ -503,8 +511,8 @@
             near_block(kind, k, o).start()
             own[o, span] = dot(x_ref[pl.ds(OWN, rows), :], w_ref[o])
 
-    def mixout_far(h, part):
-        far("mix", mixed, wb, h, part)
+    def mixout_far(h, part, sides=(DIAG, TWIN)):
+        far("mix", mixed, wb, h, part, sides)
 
     def mixout_near(h):
         near("mix", mixed, wb, h)
@@ -555,14 +563,109 @@
 
         lax.fori_loop(0, count // tm, unit, 0)
 
+    tm = SEQ
+    C, D, Q, S = range(4)
+
+    def low_parts(h):
+        return [(k, o, p) for k, o in numbered(h) for p in lowered[h]]
+
+    def add_near():
+        def unit(i, _):
+            m = pl.ds(pl.multiple_of(i * 32, 32), 32)
+            for b in range(n):
+                own[b, m] = (
+                    residual_scale * fst[m, pl.ds(b * nc, nc)].astype(F32)
+                    + own[b, m]
+                    + precv[b, m].astype(F32)
+                )
+            return 0
+
+        lax.fori_loop(0, rows // 32, unit, 0)
+
+    def add_across(h):
+        for k, o, part in low_parts(h):
+            across_block("low", k, o, part).wait_recv()
+        for k, o in numbered(h):
+
+            def unit(i, _):
+                m = pl.ds(pl.multiple_of(i * tm, tm), tm)
+                x = own[o, m] + xrecv[o, m].astype(F32)
+                own[o, m] = x
+                lanes = x[:, :128] + x[:, 128:]
+                stats[S, m] = lanes if k == 0 else stats[S, m] + lanes
+                return 0
+
+            lax.fori_loop(0, rows // tm, unit, 0)
+
+    def center():
+        but_last = [o for h in range(half) for o in owners(h)]
+
+        def unit(i, _):
+            m = pl.ds(pl.multiple_of(i * tm, tm), tm)
+            c = jnp.sum(stats[S, m], axis=-1, keepdims=True) / ((n - 1) * nc)
+            shift = square = None
+            for o in but_last:
+                x = own[o, m] - c
+                y = x * x
+                lanes, squares = x[:, :128] + x[:, 128:], y[:, :128] + y[:, 128:]
+                shift = lanes if shift is None else shift + lanes
+                square = squares if square is None else square + squares
+            stats[C, m] = jnp.broadcast_to(c, (tm, 128))
+            stats[D, m] = shift
+            stats[Q, m] = square
+            return 0
+
+        lax.fori_loop(0, rows // tm, unit, 0)
+
+    def finish():
+        for k, o, part in low_parts(half):
+            across_block("low", k, o, part).wait_recv()
+        tail = owners(half)[0]
+
+        def measure(i, _):
+            m = pl.ds(pl.multiple_of(i * tm, tm), tm)
+            value = own[tail, m] + xrecv[tail, m].astype(F32)
+            own[tail, m] = value
+            c = stats[C, m]
+            x, y = value[:, :128] - c, value[:, 128:] - c
+            shift = jnp.sum(stats[D, m] + (x + y), axis=-1, keepdims=True) / d
+            square = jnp.sum(stats[Q, m] + (x * x + y * y), axis=-1, keepdims=True) / d
+            spread = jnp.maximum(square - shift * shift, 0.0)
+            stats[C, m] = c + shift
+            stats[S, m] = jnp.broadcast_to(lax.rsqrt(spread + norm_epsilon), (tm, 128))
+            return 0
+
+        lax.fori_loop(0, rows // tm, measure, 0)
+
+        def apply(i, _):
+            m = pl.ds(pl.multiple_of(i * 32, 32), 32)
+            mean, scale = stats[C, m], stats[S, m]
+            for b in range(n):
+                for half_block in range(nc // 128):
+                    part = pl.ds(half_block * 128, 128)
+                    cols = pl.ds(b * nc + half_block * 128, 128)
+                    out_ref[m, cols] = (
+                        (own[b, m, part] - mean) * scale * norm2_ref[:, cols]
+                    ).astype(BF)
+            return 0
+
+        lax.fori_loop(0, rows // 32, apply, 0)
+
     def near_first(p):
         return mate_copy(
-            ("near", p), fst.at[pl.ds(p * seq, seq)], fst.at[pl.ds(MATE + p * seq, seq)]
+            ("near", p),
+            fst.at[pl.ds(p * seq, seq)],
+            fst.at[pl.ds(MATE + p * seq, seq)],
+            "near",
+            "near",
         )
 
     def twin_first(p):
         return across_copy(
-            ("twin", p), fst.at[pl.ds(p * seq, seq)], fst.at[pl.ds(TWIN + p * seq, seq)]
+            ("twin", p),
+            fst.at[pl.ds(p * seq, seq)],
+            fst.at[pl.ds(TWIN + p * seq, seq)],
+            "first",
         )
 
     def diag_first(p):
@@ -570,15 +673,14 @@
             ("diag", p),
             fst.at[pl.ds(TWIN + p * seq, seq)],
             fst.at[pl.ds(DIAG + p * seq, seq)],
+            "diag",
         )
 
     def take_near_sums(kind):
-        for k, o in every:
-            near_block(kind, k, o).wait_recv()
+        mate_whole(precv.at[:, pl.ds(0, rows)], kind, (kind, "near")).wait_recv()
 
     def make_first(part):
-        for k, o in every:
-            across_block("mix", k, o, part).wait_recv()
+        across_whole(xrecv.at[:, pl.ds(*part)], "mix", ("mix", part)).wait_recv()
         start, count = part
         for p in range(start // seq, (start + count) // seq):
             norm(tok, norm1_ref, fst, p * seq, seq)
@@ -586,19 +688,15 @@
             near_first(p).start()
 
     def take_near():
-        for p in range(pieces):
-            near_first(p).wait_recv()
+        mate_whole(fst.at[pl.ds(MATE, rows)], "near", "near").wait_recv()
 
     def relay_first(p):
         twin_first(p).wait_recv()
         diag_first(p).start()
 
     def free_sends():
-        for k, o in every:
-            near_block("mix", k, o).wait_send()
-            for part in (EARLY, LATE):
-                far_block("mix", k, o, part).wait_send()
-                across_block("mix", k, o, part).wait_send()
+        mate_whole(psend, "mix").wait_send()
+        across_whole(xsend, "mix").wait_send()
 
     plan = {}
 
@@ -610,25 +708,28 @@
 
     last = half - 1
 
-    after(0, 1, 0, do(relay_tokens, 0), do(project_near, 0), do(project_far, 0, ALL))
+    after(0, 1, 0, do(relay_tokens, 0), do(project_near, 0), do(project_far, 0))
     for h in range(1, last):
         after(0, h, 1, do(relay_tokens, h))
-        after(0, h + 1, 0, do(project_near, h), do(project_far, h, ALL))
+        after(0, h + 1, 0, do(project_near, h), do(project_far, h))
     after(0, last, 1, do(relay_tokens, last), do(relay_tokens, half))
-    after(0, last, 1, do(project_near, last), do(project_far, last, ALL))
-    after(0, half, 0, do(project_far, half, EARLY), do(mix, TWIN, EARLY))
-    after(0, half, 0, do(mixout_far, 0, EARLY))
-    after(1, 1, 0, do(project_far, half, LATE), do(mix_pass, 0, EARLY), do(mix, TWIN, LATE))
-    after(1, 1, 1, do(mixout_far, 1, EARLY))
+    after(0, last, 1, do(project_near, last), do(project_far, last))
+    after(0, half, 0, do(take_diag_tokens, half))
+    for side in (DIAG, TWIN):
+        after(0, half, 0, do(project, half, side, EARLY, 1), do(mix, side, EARLY, 1))
+        after(0, half, 0, do(mixout_far, 0, EARLY, (side,)))
+    after(0, half, 0, do(mix_pass, 0, EARLY))
+    after(1, 1, 0, do(project, half, TWIN, LATE), do(mix, TWIN, LATE), do(mixout_far, 0, LATE))
+    after(1, 1, 1, do(mixout_far, 1, EARLY), do(mix_pass, 0, LATE))
     after(1, 2, 0, do(mix_pass, 1, EARLY))
     after(1, 2, 1, do(mixout_far, 2, EARLY))
     after(1, 3, 0, do(mix_pass, 2, EARLY), do(project_near, half))
     for h in range(3, half):
         after(1, h, 1, do(mixout_far, h, EARLY))
         after(1, h + 1, 0, do(mix_pass, h, EARLY))
-    after(1, half, 0, do(mixout_far, half, EARLY), do(mixout_far, 0, LATE))
+    after(1, half, 0, do(mixout_far, half, EARLY), do(mixout_far, 1, LATE))
     after(1, half, 0, do(mix_pass, half, EARLY))
-    for h in range(1, half + 1):
+    for h in range(2, half + 1):
         after(1, half, 0, do(mixout_far, h, LATE), do(mix_pass, h - 1, LATE))
     after(1, half, 0, do(mix, OWN, ALL), do(mix_pass, half, LATE))
     after(2, 1, 0, *[do(mixout_near, h) for h in range(half + 1)])
@@ -657,26 +758,35 @@
                 work()
 
     take_near_sums("low")
-    for kind, k, o, part in used:
-        if kind == "low":
-            across_block(kind, k, o, part).wait_recv()
-    outs = []
-    for p in range(pieces):
-        span = pl.ds(p * seq, seq)
-        norm(fst, norm2_ref, stage, p * seq, seq)
-        outs.append(pltpu.make_async_copy(stage.at[span], out_ref.at[span], load_sem.at[p]))
-        outs[p].start()
-
-    for key, copy in mate_copies.items():
-        if key[0] != "mix":
-            copy.wait_send()
-    for key, copy in across_copies.items():
-        if key[0] != "mix":
-            copy.wait_send()
-    for key in copies:
-        copies[key].wait_send()
-    for copy in outs:
-        copy.wait()
+    add_near()
+    for h in range(half):
+        add_across(h)
+    center()
+    finish()
+
+    mate_whole(tok.at[pl.ds(0, both)], "tok").wait_send()
+    for group in ("near", "diag"):
+        mate_whole(fst.at[pl.ds(0, rows)], group).wait_send()
+    mate_whole(psend, "low").wait_send()
+    across_whole(tok.at[pl.ds(0, rows)], "tok").wait_send()
+    across_whole(fst.at[pl.ds(0, rows)], "first").wait_send()
+    across_whole(xsend, "low").wait_send()
+    for ti, ref in enumerate(
+        (
+            wa.at[pl.ds(0, (n - 1) * ks)],
+            wb.at[pl.ds(0, n - 1)],
+            wc.at[pl.ds(0, (n - 1) * ks)],
+            wd.at[pl.ds(0, n - 1)],
+        )
+    ):
+        pltpu.make_async_remote_copy(
+            src_ref=ref,
+            dst_ref=ref,
+            send_sem=ring_send.at[ti],
+            recv_sem=ring_recv.at[0],
+            device_id=right,
+            device_id_type=MESH,
+        ).wait_send()
 
 
 def fits(mesh, args):
@@ -727,11 +837,11 @@
     anywhere = pl.BlockSpec(memory_space=pl.ANY)
     vmem = pl.BlockSpec(memory_space=pltpu.VMEM)
     messages = 4 * (2 * n - 2)
-    pairs = 1 + n + 6 * n + 2 * (rows // SEQ)
-    crosses = n + 4 * n + rows // SEQ
+    pairs = 4 * n + 7 + rows // SEQ
+    crosses = 2 + n + n + 3 + rows // SEQ
     return pl.pallas_call(
         functools.partial(layer_kernel, n),
-        out_shape=jax.ShapeDtypeStruct((rows, d), BF),
+        out_shape=pltpu.VMEM((rows, d), BF),
         in_specs=[
             anywhere,
             anywhere,
@@ -744,7 +854,7 @@
             anywhere,
             vmem,
         ],
-        out_specs=anywhere,
+        out_specs=vmem,
         scratch_shapes=[
             pltpu.VMEM((n * ks, 3 * wch), BF),
             pltpu.VMEM((n, wch, nc), BF),
@@ -760,17 +870,17 @@
             pltpu.VMEM((n, rows, nc), BF),
             pltpu.VMEM((2 * both, d), BF),
             pltpu.VMEM((2 * both, ff), BF),
-            pltpu.VMEM((rows, d), BF),
+            pltpu.VMEM((4, rows, 128), F32),
             pltpu.SemaphoreType.DMA((8,)),
+            pltpu.SemaphoreType.DMA((4,)),
             pltpu.SemaphoreType.DMA((messages,)),
-            pltpu.SemaphoreType.DMA((messages,)),
+            pltpu.SemaphoreType.DMA((5,)),
             pltpu.SemaphoreType.DMA((pairs,)),
-            pltpu.SemaphoreType.DMA((pairs,)),
-            pltpu.SemaphoreType.DMA((crosses,)),
+            pltpu.SemaphoreType.DMA((4,)),
             pltpu.SemaphoreType.DMA((crosses,)),
         ],
         compiler_params=pltpu.CompilerParams(
-            collective_id=0, has_side_effects=True, vmem_limit_bytes=67043328
+            collective_id=0, has_side_effects=True, vmem_limit_bytes=62 * 2**20
         ),
         name="layer",
     )(

time: 169 us -> 161 us (0.953)
  Pallas kernels: 166 us -> 160 us
    pallas_call x1, Pallas kernels: 166 us -> 160 us  [fused(): pl.pallas_call(functools.partial(layer_kernel, n), out_shape=pltpu.VMEM((...]
where the time goes in v3:
time: 161 us
  Pallas kernels  160 us (99%)
    pallas_call x1, Pallas kernels, fused(): pl.pallas_call(functools.partial(layer_kernel, n), out_shape=pltpu.VMEM((...  160 us

profile of v3, /device:TPU:0, one launch (start us, length us, event | category | flops | bytes accessed | tf_op | source)
XLA Modules:
  0.0 160.7 jit_solution(13639629351816844403)
XLA Ops:
  0.0 159.5 %layer.1 = bf16[384,2048]{1,0:T(8,128)(2,1)S(1)} custom-call(bf16[384,2048]{1,0:T(8,128)(2,1)} %tokens_hbm.1, f32[256,768]{1,0:T(8,128)} %outer_hbm.1, f32[256,768]{1,0:T(8,128)} %inner_hbm.1, f32[256,768]{1,0:T(8,128)} %value_hbm.1, f32[3,768]{1,0:T(4,128)} %taps_ref.1, f32[768,256]{1,0:T(8,128)} %mix_hbm.1, f32[1,2048]{1,0:T(1,128)} %bitcast.2, ...), custom_call_target="tpu_custom_call" | custom-call | tf_op jit(solution)/shard_map/layer/pallas_call | solution.py:842
  159.5 1.1 copy.12

commit v4 on v3

--- a/solution.py
+++ b/solution.py
@@ -138,7 +138,7 @@
     both = 2 * rows
     d = tokens_hbm.shape[1]
     ks = outer_hbm.shape[0]
-    wch = wb.shape[1]
+    wch = wb.shape[1] // 2
     ff = wc.shape[1]
     nc = wb.shape[2]
     OWN, TWIN, MATE, DIAG = 0, rows, 2 * rows, 3 * rows
@@ -167,6 +167,16 @@
         return [(0 if h == 0 else 2 * h - 1 + k, o) for k, o in enumerate(owners(h))]
 
     every = [item for h in range(half + 1) for item in numbered(h)]
+
+    units = [((f, 0), (f, 1))]
+    for h in range(1, half):
+        a, b = owners(h)
+        units += [((a, 0), (b, 1)), ((a, 1), (b, 0))]
+    units.append(tuple((o, j) for o in owners(half) for j in range(2)))
+    lane = nc // 2
+
+    def columns(o, j):
+        return pl.ds(pl.multiple_of(o * nc + j * lane, lane), lane)
 
     mine = pl.multiple_of(r * ff, 128)
     share_at = pl.multiple_of(r * wch, 128)
@@ -182,7 +192,7 @@
     ]
     loads += [
         pltpu.make_async_copy(
-            mix_hbm.at[pl.ds(share_at, wch)], own.at[0, pl.ds(0, wch)], load_sem.at[3]
+            mix_hbm, own.at[0, pl.ds(0, 2 * wch)], load_sem.at[3]
         ),
         pltpu.make_async_copy(
             up_hbm.at[:, pl.ds(mine, ff)],
@@ -204,8 +214,8 @@
                 load_sem.at[7],
             )
         )
-    for load in loads[:3]:
-        load.start()
+    for i in (3, 0, 1, 2):
+        loads[i].start()
 
     barrier = pltpu.get_barrier_semaphore()
     for device in (right, left, across, mate):
@@ -245,14 +255,12 @@
 
     def piece(ti, which, owner):
         if ti == 0:
-            u = ks // 2
-            return wa.at[pl.ds(pl.multiple_of(owner * ks + which * u, 16), u)]
-        if ti == 1:
-            return wb.at[owner, pl.ds(which * (wch // 2), wch // 2)]
-        if ti == 2:
-            u = ks // 2
-            return wc.at[pl.ds(pl.multiple_of(owner * ks + which * u, 16), u)]
-        return wd.at[owner, pl.ds(which * (ff // 2), ff // 2)]
+            u = wch // 2
+            return wb.at[owner, pl.ds(pl.multiple_of(share_at + which * u, 16), u)]
+        u = ks // 2
+        if ti < 3:
+            return (wa, wc)[ti - 1].at[pl.ds(pl.multiple_of(owner * ks + which * u, 16), u)]
+        return wd.at[owner, which]
 
     per = 4 * half - 2
     index = {}
@@ -343,29 +351,35 @@
     share = mate_copy("share", tokens_hbm, tok.at[pl.ds(MATE, rows)], "tok")
     for k, o in every:
         twin_tokens(k, o).start()
+    loads[3].wait()
+    wb[f] = own[0, pl.ds(0, 2 * wch)].astype(BF)
+    send(0, "Rq", 1)
+    send(0, "Lp", 1)
+    send(0, "Rp", 1)
+    send(0, "Lq", 1)
+    for load in loads[4:]:
+        load.start()
+    share.start()
     for i in range(3):
         loads[i].wait()
         wa[pl.ds(pl.multiple_of(f * ks, 16), ks), pl.ds(i * wch, wch)] = acc[
             pl.ds(i * ks, ks), pl.ds(0, wch)
         ].astype(BF)
-    send(0, "Rq", 1)
-    send(0, "Lp", 1)
-    send(0, "Rp", 1)
-    send(0, "Lq", 1)
-    for load in loads[3:]:
-        load.start()
-    share.start()
-    loads[3].wait()
-    wb[f] = own[0, pl.ds(0, wch)].astype(BF)
     loads[4].wait()
     wc[pl.ds(pl.multiple_of(f * ks, 16), ks), :] = acc[
         pl.ds(3 * ks, ks), pl.ds(0, ff)
     ].astype(BF)
     loads[5].wait()
-    wd[f, pl.ds(0, first_down)] = own[1, pl.ds(0, first_down)].astype(BF)
+    for j in range(2):
+        wd[f, j, pl.ds(0, first_down)] = own[
+            1, pl.ds(0, first_down), pl.ds(j * lane, lane)
+        ].astype(BF)
     if rest_down:
         loads[7].wait()
-        wd[f, pl.ds(first_down, rest_down)] = own[2, pl.ds(0, rest_down)].astype(BF)
+        for j in range(2):
+            wd[f, j, pl.ds(first_down, rest_down)] = own[
+                2, pl.ds(0, rest_down), pl.ds(j * lane, lane)
+            ].astype(BF)
     loads[6].wait()
     share.wait_recv()
 
@@ -374,6 +388,11 @@
     pieces = rows // seq
     most = pieces - 1
     EARLY, LATE, ALL = (0, most * seq), (most * seq, seq), (0, rows)
+
+    def cross_wb(h):
+        for k, o in numbered(h):
+            ref = wb.at[o, pl.ds(share_at, wch)]
+            across_copy(("wb", k), ref, ref, "wb", "wb").start()
 
     def relay_tokens(h):
         for k, o in numbered(h):
@@ -432,7 +451,7 @@
             after = jnp.where(place < seq - 1, pltpu.roll(p, seq - 1, 0), 0.0)
             taps = taps_ref[:, pl.ds(pl.multiple_of(share_at + c, tc), tc)]
             conv = taps[0:1] * before + taps[1:2] * p + taps[2:3] * after
-            mixed[m, pl.ds(c, tc)] = (o * conv).astype(BF)
+            mixed[m, pl.ds(pl.multiple_of(share_at + c, tc), tc)] = (o * conv).astype(BF)
             return 0
 
         lax.fori_loop(0, sides * seqs * (wch // tc), unit, 0)
@@ -471,63 +490,79 @@
             diag_first(p).wait_recv()
         raise_part(count, start, TWIN, both, range(half + 1), True, True)
 
-    def far_block(kind, k, o, part):
+    def send_mixed(p):
+        for there, here in ((TWIN, OWN), (DIAG, MATE)):
+            across_copy(
+                ("mixed", there, p),
+                mixed.at[pl.ds(there + p * seq, seq), pl.ds(share_at, wch)],
+                mixed.at[pl.ds(here + p * seq, seq), pl.ds(share_at, wch)],
+                "mixed",
+                ("mixed", p),
+            ).start()
+
+    def mix_sums(p):
+        span = pl.ds(p * seq, seq)
+        return mate_copy(("mix", p), psend.at[:, span], precv.at[:, span], "mix")
+
+    def mixout(p):
+        span = pl.ds(p * seq, seq)
+        if p == 0:
+            across_whole(wb.at[pl.ds(0, n - 1), pl.ds(0, wch)], "wb", "wb").wait_recv()
+        across_whole(
+            mixed.at[pl.ds(0, 2 * seq), pl.ds(0, wch)], "mixed", ("mixed", p)
+        ).wait_recv()
+
+        def theirs(b, _):
+            psend[b, span] = dot(mixed[pl.ds(MATE + p * seq, seq), :], wb[b]).astype(BF)
+            return 0
+
+        lax.fori_loop(0, n, theirs, 0)
+        mix_sums(p).start()
+
+        def ours(b, _):
+            own[b, span] = dot(mixed[pl.ds(OWN + p * seq, seq), :], wb[b])
+            return 0
+
+        lax.fori_loop(0, n, ours, 0)
+
+    def far_block(u, part):
         span = pl.ds(rows + part[0], part[1])
-        return mate_copy((kind, k, part), psend.at[o, span], precv.at[o, span], kind)
-
-    def near_block(kind, k, o):
+        return mate_copy(("low", u, part), psend.at[u, span], precv.at[u, span], "low")
+
+    def near_block(u):
         span = pl.ds(0, rows)
-        return mate_copy((kind, k), psend.at[o, span], precv.at[o, span], kind, (kind, "near"))
-
-    def across_block(kind, k, o, part):
+        return mate_copy(
+            ("low", u), psend.at[u, span], precv.at[u, span], "low", ("low", "near")
+        )
+
+    def across_block(u, part):
         span = pl.ds(*part)
-        arrival = ("mix", part) if kind == "mix" else None
-        return across_copy((kind, k, part), xsend.at[o, span], xrecv.at[o, span], kind, arrival)
-
-    lowered = {h: [EARLY, LATE] if h < 2 else [ALL] for h in range(half + 1)}
-
-    def far(kind, x_ref, w_ref, h, part, sides=(DIAG, TWIN)):
+        return across_copy(("low", u, part), xsend.at[u, span], xrecv.at[u, span], "low")
+
+    def down(u):
+        return jnp.concatenate([wd[o, j] for o, j in units[u]], axis=1)
+
+    def lower_far(u, part):
         start, count = part
-        for k, o in numbered(h):
-            span = pl.ds(rows + start, count)
-            if DIAG in sides:
-                psend[o, span] = dot(x_ref[pl.ds(DIAG + start, count), :], w_ref[o]).astype(BF)
-                far_block(kind, k, o, part).start()
-            if TWIN in sides:
-                own[o, span] = dot(x_ref[pl.ds(TWIN + start, count), :], w_ref[o])
-
-    def pass_far(kind, h, part):
+        span = pl.ds(rows + start, count)
+        psend[u, span] = dot(hid[pl.ds(DIAG + start, count), :], down(u)).astype(BF)
+        far_block(u, part).start()
+        own[u, span] = dot(hid[pl.ds(TWIN + start, count), :], down(u))
+
+    def low_pass(u, part):
         start, count = part
-        for k, o in numbered(h):
-            far_block(kind, k, o, part).wait_recv()
-            span = pl.ds(rows + start, count)
-            xsend[o, pl.ds(start, count)] = (own[o, span] + precv[o, span].astype(F32)).astype(BF)
-            across_block(kind, k, o, part).start()
-
-    def near(kind, x_ref, w_ref, h):
+        far_block(u, part).wait_recv()
+        span = pl.ds(rows + start, count)
+        xsend[u, pl.ds(start, count)] = (own[u, span] + precv[u, span].astype(F32)).astype(BF)
+        across_block(u, part).start()
+
+    def lower_near(u):
         span = pl.ds(0, rows)
-        for k, o in numbered(h):
-            psend[o, span] = dot(x_ref[pl.ds(MATE, rows), :], w_ref[o]).astype(BF)
-            near_block(kind, k, o).start()
-            own[o, span] = dot(x_ref[pl.ds(OWN, rows), :], w_ref[o])
-
-    def mixout_far(h, part, sides=(DIAG, TWIN)):
-        far("mix", mixed, wb, h, part, sides)
-
-    def mixout_near(h):
-        near("mix", mixed, wb, h)
-
-    def lower_far(h, part):
-        far("low", hid, wd, h, part)
-
-    def lower_near(h):
-        near("low", hid, wd, h)
-
-    def mix_pass(h, part):
-        pass_far("mix", h, part)
-
-    def low_pass(h, part):
-        pass_far("low", h, part)
+        psend[u, span] = dot(hid[pl.ds(MATE, rows), :], down(u)).astype(BF)
+        near_block(u).start()
+        own[u, span] = dot(hid[pl.ds(OWN, rows), :], down(u))
+
+    lowered = [[EARLY, LATE] if u < 3 else [ALL] for u in range(n)]
 
     def norm(base_ref, gain_ref, dest_ref, start, count):
         tm = 32
@@ -541,9 +576,7 @@
                     * base_ref[pl.ds(m, tm), pl.ds(b * nc, nc)].astype(F32)
                     + own[b, pl.ds(m, tm)]
                 )
-                for term in (precv, xrecv):
-                    part = part + term[b, pl.ds(m, tm)].astype(F32)
-                parts.append(part)
+                parts.append(part + precv[b, pl.ds(m, tm)].astype(F32))
             total = parts[0]
             for b in range(1, n):
                 total = total + parts[b]
@@ -566,51 +599,47 @@
     tm = SEQ
     C, D, Q, S = range(4)
 
-    def low_parts(h):
-        return [(k, o, p) for k, o in numbered(h) for p in lowered[h]]
-
     def add_near():
         def unit(i, _):
             m = pl.ds(pl.multiple_of(i * 32, 32), 32)
-            for b in range(n):
-                own[b, m] = (
-                    residual_scale * fst[m, pl.ds(b * nc, nc)].astype(F32)
-                    + own[b, m]
-                    + precv[b, m].astype(F32)
-                )
+            for u in range(n):
+                for i, place in enumerate(units[u]):
+                    part = pl.ds(i * lane, lane)
+                    own[u, m, part] = (
+                        residual_scale * fst[m, columns(*place)].astype(F32)
+                        + own[u, m, part]
+                        + precv[u, m, part].astype(F32)
+                    )
             return 0
 
         lax.fori_loop(0, rows // 32, unit, 0)
 
-    def add_across(h):
-        for k, o, part in low_parts(h):
-            across_block("low", k, o, part).wait_recv()
-        for k, o in numbered(h):
-
-            def unit(i, _):
-                m = pl.ds(pl.multiple_of(i * tm, tm), tm)
-                x = own[o, m] + xrecv[o, m].astype(F32)
-                own[o, m] = x
-                lanes = x[:, :128] + x[:, 128:]
-                stats[S, m] = lanes if k == 0 else stats[S, m] + lanes
-                return 0
-
-            lax.fori_loop(0, rows // tm, unit, 0)
+    def add_across(u):
+        for part in lowered[u]:
+            across_block(u, part).wait_recv()
+
+        def unit(i, _):
+            m = pl.ds(pl.multiple_of(i * tm, tm), tm)
+            x = own[u, m] + xrecv[u, m].astype(F32)
+            own[u, m] = x
+            lanes = x[:, :lane] + x[:, lane:]
+            stats[S, m] = lanes if u == 0 else stats[S, m] + lanes
+            return 0
+
+        lax.fori_loop(0, rows // tm, unit, 0)
 
     def center():
-        but_last = [o for h in range(half) for o in owners(h)]
-
         def unit(i, _):
             m = pl.ds(pl.multiple_of(i * tm, tm), tm)
             c = jnp.sum(stats[S, m], axis=-1, keepdims=True) / ((n - 1) * nc)
             shift = square = None
-            for o in but_last:
-                x = own[o, m] - c
+            for u in range(n - 1):
+                x = own[u, m] - c
                 y = x * x
-                lanes, squares = x[:, :128] + x[:, 128:], y[:, :128] + y[:, 128:]
+                lanes, squares = x[:, :lane] + x[:, lane:], y[:, :lane] + y[:, lane:]
                 shift = lanes if shift is None else shift + lanes
                 square = squares if square is None else square + squares
-            stats[C, m] = jnp.broadcast_to(c, (tm, 128))
+            stats[C, m] = jnp.broadcast_to(c, (tm, lane))
             stats[D, m] = shift
             stats[Q, m] = square
             return 0
@@ -618,21 +647,21 @@
         lax.fori_loop(0, rows // tm, unit, 0)
 
     def finish():
-        for k, o, part in low_parts(half):
-            across_block("low", k, o, part).wait_recv()
-        tail = owners(half)[0]
+        tail = n - 1
+        for part in lowered[tail]:
+            across_block(tail, part).wait_recv()
 
         def measure(i, _):
             m = pl.ds(pl.multiple_of(i * tm, tm), tm)
             value = own[tail, m] + xrecv[tail, m].astype(F32)
             own[tail, m] = value
             c = stats[C, m]
-            x, y = value[:, :128] - c, value[:, 128:] - c
+            x, y = value[:, :lane] - c, value[:, lane:] - c
             shift = jnp.sum(stats[D, m] + (x + y), axis=-1, keepdims=True) / d
             square = jnp.sum(stats[Q, m] + (x * x + y * y), axis=-1, keepdims=True) / d
             spread = jnp.maximum(square - shift * shift, 0.0)
             stats[C, m] = c + shift
-            stats[S, m] = jnp.broadcast_to(lax.rsqrt(spread + norm_epsilon), (tm, 128))
+            stats[S, m] = jnp.broadcast_to(lax.rsqrt(spread + norm_epsilon), (tm, lane))
             return 0
 
         lax.fori_loop(0, rows // tm, measure, 0)
@@ -640,13 +669,11 @@
         def apply(i, _):
             m = pl.ds(pl.multiple_of(i * 32, 32), 32)
             mean, scale = stats[C, m], stats[S, m]
-            for b in range(n):
-                for half_block in range(nc // 128):
-                    part = pl.ds(half_block * 128, 128)
-                    cols = pl.ds(b * nc + half_block * 128, 128)
-                    out_ref[m, cols] = (
-                        (own[b, m, part] - mean) * scale * norm2_ref[:, cols]
-                    ).astype(BF)
+            for u in range(n):
+                for i, place in enumerate(units[u]):
+                    cols = columns(*place)
+                    value = own[u, m, pl.ds(i * lane, lane)]
+                    out_ref[m, cols] = ((value - mean) * scale * norm2_ref[:, cols]).astype(BF)
             return 0
 
         lax.fori_loop(0, rows // 32, apply, 0)
@@ -676,16 +703,14 @@
             "diag",
         )
 
-    def take_near_sums(kind):
-        mate_whole(precv.at[:, pl.ds(0, rows)], kind, (kind, "near")).wait_recv()
-
-    def make_first(part):
-        across_whole(xrecv.at[:, pl.ds(*part)], "mix", ("mix", part)).wait_recv()
-        start, count = part
-        for p in range(start // seq, (start + count) // seq):
-            norm(tok, norm1_ref, fst, p * seq, seq)
-            twin_first(p).start()
-            near_first(p).start()
+    def take_near_sums():
+        mate_whole(precv.at[:, pl.ds(0, rows)], "low", ("low", "near")).wait_recv()
+
+    def make_first(p):
+        mix_sums(p).wait_recv()
+        norm(tok, norm1_ref, fst, p * seq, seq)
+        twin_first(p).start()
+        near_first(p).start()
 
     def take_near():
         mate_whole(fst.at[pl.ds(MATE, rows)], "near", "near").wait_recv()
@@ -695,8 +720,7 @@
         diag_first(p).start()
 
     def free_sends():
-        mate_whole(psend, "mix").wait_send()
-        across_whole(xsend, "mix").wait_send()
+        mate_whole(psend.at[:, pl.ds(0, rows)], "mix").wait_send()
 
     plan = {}
 
@@ -708,48 +732,44 @@
 
     last = half - 1
 
-    after(0, 1, 0, do(relay_tokens, 0), do(project_near, 0), do(project_far, 0))
-    for h in range(1, last):
-        after(0, h, 1, do(relay_tokens, h))
-        after(0, h + 1, 0, do(project_near, h), do(project_far, h))
-    after(0, last, 1, do(relay_tokens, last), do(relay_tokens, half))
-    after(0, last, 1, do(project_near, last), do(project_far, last))
-    after(0, half, 0, do(take_diag_tokens, half))
-    for side in (DIAG, TWIN):
-        after(0, half, 0, do(project, half, side, EARLY, 1), do(mix, side, EARLY, 1))
-        after(0, half, 0, do(mixout_far, 0, EARLY, (side,)))
-    after(0, half, 0, do(mix_pass, 0, EARLY))
-    after(1, 1, 0, do(project, half, TWIN, LATE), do(mix, TWIN, LATE), do(mixout_far, 0, LATE))
-    after(1, 1, 1, do(mixout_far, 1, EARLY), do(mix_pass, 0, LATE))
-    after(1, 2, 0, do(mix_pass, 1, EARLY))
-    after(1, 2, 1, do(mixout_far, 2, EARLY))
-    after(1, 3, 0, do(mix_pass, 2, EARLY), do(project_near, half))
-    for h in range(3, half):
-        after(1, h, 1, do(mixout_far, h, EARLY))
-        after(1, h + 1, 0, do(mix_pass, h, EARLY))
-    after(1, half, 0, do(mixout_far, half, EARLY), do(mixout_far, 1, LATE))
-    after(1, half, 0, do(mix_pass, half, EARLY))
-    for h in range(2, half + 1):
-        after(1, half, 0, do(mixout_far, h, LATE), do(mix_pass, h - 1, LATE))
-    after(1, half, 0, do(mix, OWN, ALL), do(mix_pass, half, LATE))
-    after(2, 1, 0, *[do(mixout_near, h) for h in range(half + 1)])
-    after(2, 1, 1, do(take_near_sums, "mix"), do(make_first, EARLY))
-    after(2, 2, 1, do(make_first, LATE), do(take_near))
-    after(2, 2, 1, do(raise_near, 0), do(raise_near, 1))
+    for h in range(1, half):
+        after(0, h, 1, do(cross_wb, h))
+    after(0, half, 0, do(cross_wb, half))
+    after(0, half, 0, do(relay_tokens, 0), do(project_near, 0), do(project_far, 0))
+    for h in range(1, half):
+        after(1, h, 0, do(relay_tokens, h))
+        after(1, h, 1, do(project_near, h), do(project_far, h))
+    after(1, last, 0, do(relay_tokens, half))
+    after(1, half, 0, do(take_diag_tokens, half))
+    after(1, half, 0, do(project, half, TWIN, EARLY), do(mix, TWIN, EARLY))
+    for p in range(most):
+        after(1, half, 0, do(send_mixed, p))
+    after(1, half, 0, do(project, half, TWIN, LATE), do(mix, TWIN, LATE), do(send_mixed, most))
+    after(1, half, 0, do(project_near, half), do(mix, OWN, ALL))
+    after(2, 1, 0, do(mixout, 0))
+    after(2, 1, 1, do(make_first, 0), do(mixout, 1), do(make_first, 1))
+    for p in range(2, pieces):
+        after(2, 2, 0, do(mixout, p), do(make_first, p))
+    after(2, 2, 1, do(take_near), do(raise_near, 0), do(raise_near, 1))
     after(2, 3, 0, do(raise_near, 2), do(free_sends))
     for h in range(3, half):
         after(2, h, 1, do(raise_near, h))
-    after(2, half, 0, do(relay_first, 0), do(raise_near, half))
+    after(2, last, 1, do(relay_first, 0))
+    after(2, half, 0, do(raise_near, half), do(lower_near, 0))
     for p in range(1, most):
-        after(3, 1, 0, do(relay_first, p))
-    after(3, 1, 0, do(lower_near, 0), do(raise_far, EARLY))
-    after(3, 1, 1, do(lower_far, 0, EARLY), do(lower_far, 1, EARLY), do(low_pass, 0, EARLY))
-    after(3, 1, 1, do(low_pass, 1, EARLY), do(relay_first, most), do(raise_far, LATE))
-    after(3, 2, 0, do(lower_far, 0, LATE), do(lower_far, 1, LATE))
-    after(3, 2, 0, do(low_pass, 0, LATE), do(low_pass, 1, LATE), do(lower_near, 1))
-    for h in range(2, half):
-        after(3, h, 1, do(lower_far, h, ALL), do(low_pass, h, ALL), do(lower_near, h))
-    after(3, half, 0, do(lower_far, half, ALL), do(low_pass, half, ALL), do(lower_near, half))
+        after(2, half, 0, do(relay_first, p))
+    after(2, half, 0, do(raise_far, EARLY))
+    after(3, 1, 0, do(lower_far, 0, EARLY), do(lower_far, 1, EARLY))
+    after(3, 1, 0, do(low_pass, 0, EARLY), do(low_pass, 1, EARLY), do(relay_first, most))
+    after(3, 1, 1, do(lower_far, 2, EARLY), do(low_pass, 2, EARLY), do(raise_far, LATE))
+    for u in range(3):
+        after(3, 1, 1, do(lower_far, u, LATE))
+    for u in range(3):
+        after(3, 1, 1, do(low_pass, u, LATE))
+    for u in range(3, n):
+        e = (3, half, 0) if u == n - 1 else (3, (u + 1) // 2, (u + 1) % 2)
+        after(*e, do(lower_far, u, ALL), do(lower_near, u - 2), do(low_pass, u, ALL))
+    after(3, half, 0, do(lower_near, n - 2), do(lower_near, n - 1))
 
     for ti in range(4):
         for e in events(ti):
@@ -757,10 +777,10 @@
             for work in plan.get(e, ()):
                 work()
 
-    take_near_sums("low")
+    take_near_sums()
     add_near()
-    for h in range(half):
-        add_across(h)
+    for u in range(n - 1):
+        add_across(u)
     center()
     finish()
 
@@ -769,12 +789,14 @@
         mate_whole(fst.at[pl.ds(0, rows)], group).wait_send()
     mate_whole(psend, "low").wait_send()
     across_whole(tok.at[pl.ds(0, rows)], "tok").wait_send()
+    across_whole(wb.at[pl.ds(0, n - 1), pl.ds(0, wch)], "wb").wait_send()
+    across_whole(mixed.at[pl.ds(0, both), pl.ds(0, wch)], "mixed").wait_send()
     across_whole(fst.at[pl.ds(0, rows)], "first").wait_send()
     across_whole(xsend, "low").wait_send()
     for ti, ref in enumerate(
         (
+            wb.at[pl.ds(0, n - 1), pl.ds(0, wch)],
             wa.at[pl.ds(0, (n - 1) * ks)],
-            wb.at[pl.ds(0, n - 1)],
             wc.at[pl.ds(0, (n - 1) * ks)],
             wd.at[pl.ds(0, n - 1)],
         )
@@ -805,7 +827,7 @@
         and nc == 256
         and wch % 128 == 0
         and ff % 256 == 0
-        and wch <= 2 * rows
+        and wch <= rows
         and ff <= 4 * rows
         and ff <= 3 * wch
         and ks <= rows
@@ -837,8 +859,8 @@
     anywhere = pl.BlockSpec(memory_space=pl.ANY)
     vmem = pl.BlockSpec(memory_space=pltpu.VMEM)
     messages = 4 * (2 * n - 2)
-    pairs = 4 * n + 7 + rows // SEQ
-    crosses = 2 + n + n + 3 + rows // SEQ
+    pairs = 2 * n + 6 + 2 * (rows // SEQ)
+    crosses = 2 * n + 4 + 2 * (rows // SEQ)
     return pl.pallas_call(
         functools.partial(layer_kernel, n),
         out_shape=pltpu.VMEM((rows, d), BF),
@@ -857,12 +879,12 @@
         out_specs=vmem,
         scratch_shapes=[
             pltpu.VMEM((n * ks, 3 * wch), BF),
-            pltpu.VMEM((n, wch, nc), BF),
+            pltpu.VMEM((n, 2 * wch, nc), BF),
             pltpu.VMEM((n * ks, ff), BF),
-            pltpu.VMEM((n, ff, nc), BF),
+            pltpu.VMEM((n, 2, ff, nc // 2), BF),
             pltpu.VMEM((2 * both, d), BF),
             pltpu.VMEM((2 * both, 3 * wch), F32),
-            pltpu.VMEM((2 * both, wch), BF),
+            pltpu.VMEM((2 * both, 2 * wch), BF),
             pltpu.VMEM((n, both, nc), F32),
             pltpu.VMEM((n, both, nc), BF),
             pltpu.VMEM((n, both, nc), BF),
@@ -876,7 +898,7 @@
             pltpu.SemaphoreType.DMA((messages,)),
             pltpu.SemaphoreType.DMA((5,)),
             pltpu.SemaphoreType.DMA((pairs,)),
-            pltpu.SemaphoreType.DMA((4,)),
+            pltpu.SemaphoreType.DMA((5,)),
             pltpu.SemaphoreType.DMA((crosses,)),
         ],
         compiler_params=pltpu.CompilerParams(

time: 161 us -> 156 us (0.969)
  Pallas kernels: 160 us -> 155 us
    pallas_call x1, Pallas kernels: 160 us -> 155 us  [fused(): pl.pallas_call(functools.partial(layer_kernel, n), out_shape=pltpu.VMEM((...]
where the time goes in v4:
time: 156 us
  Pallas kernels  155 us (99%)
    pallas_call x1, Pallas kernels, fused(): pl.pallas_call(functools.partial(layer_kernel, n), out_shape=pltpu.VMEM((...  155 us

profile of v4, /device:TPU:0, one launch (start us, length us, event | category | flops | bytes accessed | tf_op | source)
XLA Modules:
  0.0 155.9 jit_solution(4745087447756898826)
XLA Ops:
  0.0 154.7 %layer.1 = bf16[384,2048]{1,0:T(8,128)(2,1)S(1)} custom-call(bf16[384,2048]{1,0:T(8,128)(2,1)} %tokens_hbm.1, f32[256,768]{1,0:T(8,128)} %outer_hbm.1, f32[256,768]{1,0:T(8,128)} %inner_hbm.1, f32[256,768]{1,0:T(8,128)} %value_hbm.1, f32[3,768]{1,0:T(4,128)} %taps_ref.1, f32[768,256]{1,0:T(8,128)} %mix_hbm.1, f32[1,2048]{1,0:T(1,128)} %bitcast.2, ...), custom_call_target="tpu_custom_call" | custom-call | tf_op jit(solution)/shard_map/layer/pallas_call | solution.py:864
  154.7 1.1 copy.12

commit v5 on v4

--- a/solution.py
+++ b/solution.py
@@ -529,10 +529,13 @@
         span = pl.ds(rows + part[0], part[1])
         return mate_copy(("low", u, part), psend.at[u, span], precv.at[u, span], "low")
 
+    def near_group(u):
+        return max(u - (n - 3), 0)
+
     def near_block(u):
         span = pl.ds(0, rows)
         return mate_copy(
-            ("low", u), psend.at[u, span], precv.at[u, span], "low", ("low", "near")
+            ("low", u), psend.at[u, span], precv.at[u, span], "low", ("low", near_group(u))
         )
 
     def across_block(u, part):
@@ -562,7 +565,7 @@
         near_block(u).start()
         own[u, span] = dot(hid[pl.ds(OWN, rows), :], down(u))
 
-    lowered = [[EARLY, LATE] if u < 3 else [ALL] for u in range(n)]
+    lowered = [[ALL] if 3 <= u < n - 1 else [EARLY, LATE] for u in range(n)]
 
     def norm(base_ref, gain_ref, dest_ref, start, count):
         tm = 32
@@ -599,10 +602,10 @@
     tm = SEQ
     C, D, Q, S = range(4)
 
-    def add_near():
+    def add_near(first, count):
         def unit(i, _):
             m = pl.ds(pl.multiple_of(i * 32, 32), 32)
-            for u in range(n):
+            for u in range(first, first + count):
                 for i, place in enumerate(units[u]):
                     part = pl.ds(i * lane, lane)
                     own[u, m, part] = (
@@ -646,13 +649,13 @@
 
         lax.fori_loop(0, rows // tm, unit, 0)
 
-    def finish():
+    def finish(part):
+        start, count = part
         tail = n - 1
-        for part in lowered[tail]:
-            across_block(tail, part).wait_recv()
+        across_block(tail, part).wait_recv()
 
         def measure(i, _):
-            m = pl.ds(pl.multiple_of(i * tm, tm), tm)
+            m = pl.ds(pl.multiple_of(start + i * tm, tm), tm)
             value = own[tail, m] + xrecv[tail, m].astype(F32)
             own[tail, m] = value
             c = stats[C, m]
@@ -664,10 +667,10 @@
             stats[S, m] = jnp.broadcast_to(lax.rsqrt(spread + norm_epsilon), (tm, lane))
             return 0
 
-        lax.fori_loop(0, rows // tm, measure, 0)
+        lax.fori_loop(0, count // tm, measure, 0)
 
         def apply(i, _):
-            m = pl.ds(pl.multiple_of(i * 32, 32), 32)
+            m = pl.ds(pl.multiple_of(start + i * 32, 32), 32)
             mean, scale = stats[C, m], stats[S, m]
             for u in range(n):
                 for i, place in enumerate(units[u]):
@@ -676,7 +679,7 @@
                     out_ref[m, cols] = ((value - mean) * scale * norm2_ref[:, cols]).astype(BF)
             return 0
 
-        lax.fori_loop(0, rows // 32, apply, 0)
+        lax.fori_loop(0, count // 32, apply, 0)
 
     def near_first(p):
         return mate_copy(
@@ -703,8 +706,11 @@
             "diag",
         )
 
-    def take_near_sums():
-        mate_whole(precv.at[:, pl.ds(0, rows)], "low", ("low", "near")).wait_recv()
+    def take_near_sums(first, count):
+        mate_whole(
+            precv.at[pl.ds(first, count), pl.ds(0, rows)], "low", ("low", near_group(first))
+        ).wait_recv()
+        add_near(first, count)
 
     def make_first(p):
         mix_sums(p).wait_recv()
@@ -766,23 +772,28 @@
         after(3, 1, 1, do(lower_far, u, LATE))
     for u in range(3):
         after(3, 1, 1, do(low_pass, u, LATE))
-    for u in range(3, n):
-        e = (3, half, 0) if u == n - 1 else (3, (u + 1) // 2, (u + 1) % 2)
-        after(*e, do(lower_far, u, ALL), do(lower_near, u - 2), do(low_pass, u, ALL))
-    after(3, half, 0, do(lower_near, n - 2), do(lower_near, n - 1))
+    for u in range(3, n - 1):
+        e = (3, (u + 1) // 2, (u + 1) % 2)
+        near = u - 2 if u < n - 2 else n - 3
+        after(*e, do(lower_far, u, ALL), do(lower_near, near), do(low_pass, u, ALL))
+    after(3, last, 0, do(lower_near, n - 4))
+    after(3, last, 1, do(lower_near, n - 2))
+    after(3, last, 1, do(take_near_sums, 0, n - 2))
+    for u in range(n - 3):
+        after(3, last, 1, do(add_across, u))
+    for work in (lower_far, low_pass):
+        after(3, half, 0, do(work, n - 1, EARLY), do(work, n - 1, LATE))
+    after(3, half, 0, do(lower_near, n - 1), do(take_near_sums, n - 2, 1))
+    for u in range(n - 3, n - 1):
+        after(3, half, 0, do(add_across, u))
+    after(3, half, 0, do(center), do(take_near_sums, n - 1, 1), do(finish, EARLY))
+    after(3, half, 0, do(finish, LATE))
 
     for ti in range(4):
         for e in events(ti):
             event(*e)
             for work in plan.get(e, ()):
                 work()
-
-    take_near_sums()
-    add_near()
-    for u in range(n - 1):
-        add_across(u)
-    center()
-    finish()
 
     mate_whole(tok.at[pl.ds(0, both)], "tok").wait_send()
     for group in ("near", "diag"):
@@ -859,8 +870,8 @@
     anywhere = pl.BlockSpec(memory_space=pl.ANY)
     vmem = pl.BlockSpec(memory_space=pltpu.VMEM)
     messages = 4 * (2 * n - 2)
-    pairs = 2 * n + 6 + 2 * (rows // SEQ)
-    crosses = 2 * n + 4 + 2 * (rows // SEQ)
+    pairs = 2 * n + 9 + 2 * (rows // SEQ)
+    crosses = 2 * n + 5 + 2 * (rows // SEQ)
     return pl.pallas_call(
         functools.partial(layer_kernel, n),
         out_shape=pltpu.VMEM((rows, d), BF),

time: 156 us -> 155 us (level)
  no operation moved by 1% of the time
where the time goes in v5:
time: 155 us
  Pallas kernels  154 us (99%)
    pallas_call x1, Pallas kernels, fused(): pl.pallas_call(functools.partial(layer_kernel, n), out_shape=pltpu.VMEM((...  154 us

profile of v5, /device:TPU:0, one launch (start us, length us, event | category | flops | bytes accessed | tf_op | source)
XLA Modules:
  0.0 154.7 jit_solution(15219946237581142216)
XLA Ops:
  0.0 153.6 %layer.1 = bf16[384,2048]{1,0:T(8,128)(2,1)S(1)} custom-call(bf16[384,2048]{1,0:T(8,128)(2,1)} %tokens_hbm.1, f32[256,768]{1,0:T(8,128)} %outer_hbm.1, f32[256,768]{1,0:T(8,128)} %inner_hbm.1, f32[256,768]{1,0:T(8,128)} %value_hbm.1, f32[3,768]{1,0:T(4,128)} %taps_ref.1, f32[768,256]{1,0:T(8,128)} %mix_hbm.1, f32[1,2048]{1,0:T(1,128)} %bitcast.2, ...), custom_call_target="tpu_custom_call" | custom-call | tf_op jit(solution)/shard_map/layer/pallas_call | solution.py:875
  153.6 1.1 copy.12

commit v6 on v5

--- a/solution.py
+++ b/solution.py
@@ -100,12 +100,12 @@
     outer_hbm,
     inner_hbm,
     value_hbm,
-    taps_ref,
+    taps_hbm,
     mix_hbm,
-    norm1_ref,
+    norm1_hbm,
     up_hbm,
     down_hbm,
-    norm2_ref,
+    norm2_hbm,
     out_ref,
     wa,
     wb,
@@ -122,6 +122,9 @@
     fst,
     hid,
     stats,
+    taps_ref,
+    norm1_ref,
+    norm2_ref,
     load_sem,
     ring_send,
     ring_recv,
@@ -206,6 +209,12 @@
         ),
         pltpu.make_async_copy(tokens_hbm, tok.at[pl.ds(0, rows)], load_sem.at[6]),
     ]
+    smalls = [
+        pltpu.make_async_copy(src, dst, load_sem.at[8 + i])
+        for i, (src, dst) in enumerate(
+            ((taps_hbm, taps_ref), (norm1_hbm, norm1_ref), (norm2_hbm, norm2_ref))
+        )
+    ]
     if rest_down:
         loads.append(
             pltpu.make_async_copy(
@@ -357,7 +366,7 @@
     send(0, "Lp", 1)
     send(0, "Rp", 1)
     send(0, "Lq", 1)
-    for load in loads[4:]:
+    for load in loads[4:] + smalls:
         load.start()
     share.start()
     for i in range(3):
@@ -380,7 +389,8 @@
             wd[f, j, pl.ds(first_down, rest_down)] = own[
                 2, pl.ds(0, rest_down), pl.ds(j * lane, lane)
             ].astype(BF)
-    loads[6].wait()
+    for load in [loads[6]] + smalls:
+        load.wait()
     share.wait_recv()
 
     tn = 256
@@ -875,18 +885,7 @@
     return pl.pallas_call(
         functools.partial(layer_kernel, n),
         out_shape=pltpu.VMEM((rows, d), BF),
-        in_specs=[
-            anywhere,
-            anywhere,
-            anywhere,
-            anywhere,
-            vmem,
-            anywhere,
-            vmem,
-            anywhere,
-            anywhere,
-            vmem,
-        ],
+        in_specs=[anywhere] * 10,
         out_specs=vmem,
         scratch_shapes=[
             pltpu.VMEM((n * ks, 3 * wch), BF),
@@ -904,7 +903,10 @@
             pltpu.VMEM((2 * both, d), BF),
             pltpu.VMEM((2 * both, ff), BF),
             pltpu.VMEM((4, rows, 128), F32),
-            pltpu.SemaphoreType.DMA((8,)),
+            pltpu.VMEM(conv_taps.shape, F32),
+            pltpu.VMEM((1, d), F32),
+            pltpu.VMEM((1, d), F32),
+            pltpu.SemaphoreType.DMA((11,)),
             pltpu.SemaphoreType.DMA((4,)),
             pltpu.SemaphoreType.DMA((messages,)),
             pltpu.SemaphoreType.DMA((5,)),

time: 155 us -> 154 us (level)
  no operation moved by 1% of the time
where the time goes in v6:
time: 154 us
  Pallas kernels  153 us (99%)
    pallas_call x1, Pallas kernels, fused(): pl.pallas_call(functools.partial(layer_kernel, n), out_shape=pltpu.VMEM((...  153 us

profile of v6, /device:TPU:0, one launch (start us, length us, event | category | flops | bytes accessed | tf_op | source)
XLA Modules:
  0.0 154.0 jit_solution(12306892417669778543)
XLA Ops:
  0.0 152.9 %layer.1 = bf16[384,2048]{1,0:T(8,128)(2,1)S(1)} custom-call(bf16[384,2048]{1,0:T(8,128)(2,1)} %tokens_hbm.1, f32[256,768]{1,0:T(8,128)} %outer_hbm.1, f32[256,768]{1,0:T(8,128)} %inner_hbm.1, f32[256,768]{1,0:T(8,128)} %value_hbm.1, f32[3,768]{1,0:T(4,128)} %taps_hbm.1, f32[768,256]{1,0:T(8,128)} %mix_hbm.1, f32[1,2048]{1,0:T(1,128)} %bitcast.2, ...), custom_call_target="tpu_custom_call" | custom-call | tf_op jit(solution)/shard_map/layer/pallas_call | solution.py:885
  152.9 1.1 copy.12

commit v7 on v6

--- a/solution.py
+++ b/solution.py
@@ -229,6 +229,8 @@
     barrier = pltpu.get_barrier_semaphore()
     for device in (right, left, across, mate):
         pl.semaphore_signal(barrier, inc=1, device_id=device, device_id_type=MESH)
+    loads[3].wait()
+    wb[f] = own[0, pl.ds(0, 2 * wch)].astype(BF)
     pl.semaphore_wait(barrier, 4)
 
     def copier(device, send_sems, recv_sems):
@@ -289,7 +291,7 @@
                 src, device = at(pos - (h - 1)), right
             else:
                 src, device = at(pos + (h - 1)), left
-            i = ti * per + index[kind, h]
+            i = ti % 2 * per + index[kind, h]
             ref = piece(ti, which, src)
             copies[key] = pltpu.make_async_remote_copy(
                 src_ref=ref,
@@ -358,14 +360,12 @@
         )
 
     share = mate_copy("share", tokens_hbm, tok.at[pl.ds(MATE, rows)], "tok")
-    for k, o in every:
-        twin_tokens(k, o).start()
-    loads[3].wait()
-    wb[f] = own[0, pl.ds(0, 2 * wch)].astype(BF)
     send(0, "Rq", 1)
     send(0, "Lp", 1)
     send(0, "Rp", 1)
     send(0, "Lq", 1)
+    for k, o in every:
+        twin_tokens(k, o).start()
     for load in loads[4:] + smalls:
         load.start()
     share.start()
@@ -879,7 +879,7 @@
     both = 2 * rows
     anywhere = pl.BlockSpec(memory_space=pl.ANY)
     vmem = pl.BlockSpec(memory_space=pltpu.VMEM)
-    messages = 4 * (2 * n - 2)
+    messages = 2 * (2 * n - 2)
     pairs = 2 * n + 9 + 2 * (rows // SEQ)
     crosses = 2 * n + 5 + 2 * (rows // SEQ)
     return pl.pallas_call(

time: 154 us -> 154 us (level)
  no operation moved by 1% of the time
where the time goes in v7:
time: 154 us
  Pallas kernels  153 us (99%)
    pallas_call x1, Pallas kernels, fused(): pl.pallas_call(functools.partial(layer_kernel, n), out_shape=pltpu.VMEM((...  153 us

profile of v7, /device:TPU:0, one launch (start us, length us, event | category | flops | bytes accessed | tf_op | source)
XLA Modules:
  0.0 153.7 jit_solution(2732182307445990988)
XLA Ops:
  0.0 152.6 %layer.1 = bf16[384,2048]{1,0:T(8,128)(2,1)S(1)} custom-call(bf16[384,2048]{1,0:T(8,128)(2,1)} %tokens_hbm.1, f32[256,768]{1,0:T(8,128)} %outer_hbm.1, f32[256,768]{1,0:T(8,128)} %inner_hbm.1, f32[256,768]{1,0:T(8,128)} %value_hbm.1, f32[3,768]{1,0:T(4,128)} %taps_hbm.1, f32[768,256]{1,0:T(8,128)} %mix_hbm.1, f32[1,2048]{1,0:T(1,128)} %bitcast.2, ...), custom_call_target="tpu_custom_call" | custom-call | tf_op jit(solution)/shard_map/layer/pallas_call | solution.py:885
  152.6 1.1 copy.12

commit v8 on v7

--- a/solution.py
+++ b/solution.py
@@ -575,6 +575,13 @@
         near_block(u).start()
         own[u, span] = dot(hid[pl.ds(OWN, rows), :], down(u))
 
+    def last_near(core):
+        near_block(n - 1)
+
+        @pl.when(t == core)
+        def _():
+            lower_near(n - 1)
+
     lowered = [[ALL] if 3 <= u < n - 1 else [EARLY, LATE] for u in range(n)]
 
     def norm(base_ref, gain_ref, dest_ref, start, count):
@@ -791,9 +798,10 @@
     after(3, last, 1, do(take_near_sums, 0, n - 2))
     for u in range(n - 3):
         after(3, last, 1, do(add_across, u))
-    for work in (lower_far, low_pass):
-        after(3, half, 0, do(work, n - 1, EARLY), do(work, n - 1, LATE))
-    after(3, half, 0, do(lower_near, n - 1), do(take_near_sums, n - 2, 1))
+    after(3, half, 0, do(lower_far, n - 1, EARLY), do(lower_far, n - 1, LATE))
+    after(3, half, 0, do(last_near, 1))
+    after(3, half, 0, do(low_pass, n - 1, EARLY), do(low_pass, n - 1, LATE))
+    after(3, half, 0, do(last_near, 0), do(take_near_sums, n - 2, 1))
     for u in range(n - 3, n - 1):
         after(3, half, 0, do(add_across, u))
     after(3, half, 0, do(center), do(take_near_sums, n - 1, 1), do(finish, EARLY))

time: 154 us -> 154 us (level)
  no operation moved by 1% of the time
where the time goes in v8:
time: 154 us
  Pallas kernels  153 us (99%)
    pallas_call x1, Pallas kernels, fused(): pl.pallas_call(functools.partial(layer_kernel, n), out_shape=pltpu.VMEM((...  153 us

profile of v8, /device:TPU:0, one launch (start us, length us, event | category | flops | bytes accessed | tf_op | source)
XLA Modules:
  0.0 154.2 jit_solution(12530633467780510616)
XLA Ops:
  0.0 153.1 %layer.1 = bf16[384,2048]{1,0:T(8,128)(2,1)S(1)} custom-call(bf16[384,2048]{1,0:T(8,128)(2,1)} %tokens_hbm.1, f32[256,768]{1,0:T(8,128)} %outer_hbm.1, f32[256,768]{1,0:T(8,128)} %inner_hbm.1, f32[256,768]{1,0:T(8,128)} %value_hbm.1, f32[3,768]{1,0:T(4,128)} %taps_hbm.1, f32[768,256]{1,0:T(8,128)} %mix_hbm.1, f32[1,2048]{1,0:T(1,128)} %bitcast.2, ...), custom_call_target="tpu_custom_call" | custom-call | tf_op jit(solution)/shard_map/layer/pallas_call | solution.py:893
  153.1 1.1 copy.12
